TPU v7x, 32 devices: a whole 2x2x4 slice. The times are simulated.
32 devices in a mesh: ep: 8 (over z, x), tp: 4 (over y, core).
Axes of the slice: x: 2, y: 2, z: 4, core: 2. Of those that a mesh axis runs over, the one named last changes fastest.
Arguments:
- queries: bfloat16 [4096, 1024], P('ep', 'tp'), may hold values from -6 to 6
- forget_forward_logits: bfloat16 [4096, 1024], P('ep', 'tp'), may hold values from -6 to 12
- forget_backward_logits: bfloat16 [4096, 1024], P('ep', 'tp'), may hold values from -6 to 12
- values: bfloat16 [4096, 1024], P('ep', 'tp'), may hold values from -6 to 6
- output_gate_logits: bfloat16 [4096, 1024], P('ep', 'tp'), may hold values from -6 to 6
- lower_bound_forward: float32 [1024], P('tp')
- lower_bound_backward: float32 [1024], P('tp')
- extra_log_decay: float32 [4096, 8], P('ep', 'tp'), may hold values from -2 to 0
- head_norm_scale: float32 [1024], P('tp'), may hold values from 0.1 to 1.9
- output_projection: bfloat16 [1024, 2048], P('tp'), may hold values from -0.1875 to 0.1875
- second_residual: bfloat16 [4096, 2048], P('ep'), may hold values from -6 to 6
- expert_norm_scale: float32 [2048], replicated, may hold values from 0.1 to 1.9
- routes: int32 [4096, 2], P('ep'), may hold values from 0 to 7, all different within a row; in each aligned block of 128 rows (0 to 127, 128 to 255, ...) at most 64 rows name the same one
- specialist_mixing_factor: float32 [4096, 2], P(('ep', 'tp')), may hold values from 0.1 to 1
- expert_gate_matrix: bfloat16 [8, 2048, 1024], P('ep', None, 'tp'), may hold values from -0.125 to 0.125
- expert_up_matrix: bfloat16 [8, 2048, 1024], P('ep', None, 'tp'), may hold values from -0.125 to 0.125
- expert_down_matrix: bfloat16 [8, 1024, 2048], P('ep', 'tp'), may hold values from -0.1875 to 0.1875
Outputs:
- mixer_output: bfloat16 [4096, 2048], P(('ep', 'tp'))
- routed_output: bfloat16 [4096, 2048], P(('ep', 'tp'))
Inputs may be any that keep to these rules, and one draw needn't show every extreme that they name: `routes`: in each aligned block of 128 rows no expert is named by more than 64 rows; the 2 experts of a row differ.
All inputs are finite; a program needn't handle non-finite values.
Results may differ from a plain program's by a relative error of at most 0.014.
Values may be sent and summed in bfloat16 or wider, within the bound.
No kernel may reach another device: no remote copies, remote signals or barrier semaphores. Data moves between devices by JAX's collectives and lax.ppermute only.
A program may use at most 128 MiB of HBM per device.

v0:
```python
import functools
import jax
import jax.numpy as jnp
from jax import lax
from jax.experimental import pallas as pl
from jax.experimental.pallas import tpu as pltpu
from jax.sharding import PartitionSpec as P

TOPK = 2
EPS = 1e-06
CHUNK = 128
FINE = 16
DIRECT_EP = 8
DOWN_PARTS = 2
F32 = jnp.float32
BF16 = jnp.bfloat16

NT = (((1,), (1,)), ((), ()))
TN = (((0,), (0,)), ((), ()))
VM = pl.BlockSpec(memory_space=pltpu.VMEM)
SM = pl.BlockSpec(memory_space=pltpu.SMEM)
HBM = pl.BlockSpec(memory_space=pl.ANY)


def cost(flops, moved, exps=0):
    return pl.CostEstimate(flops=int(flops), bytes_accessed=int(moved), transcendentals=int(exps))


def params():
    return pltpu.CompilerParams(vmem_limit_bytes=56 * 1024 * 1024)


def dot(a, b, dims=(((1,), (0,)), ((), ()))):
    return lax.dot_general(a, b, dims, preferred_element_type=F32)


def gate_terms(logits, bound, extra):
    wide = logits.astype(F32)
    grown = jnp.exp(-wide)
    opened = 1.0 / (1.0 + grown)
    floor = jax.nn.sigmoid(bound)
    rest = jax.nn.sigmoid(-bound)
    return rest * (grown * opened), jnp.log(floor + rest * opened) + extra


def running_sum(decay, lower):
    rows, width = decay.shape
    high = decay.astype(BF16)
    low = (decay - high.astype(F32)).astype(BF16)
    carry = jnp.zeros((1, width), F32)
    pieces = []
    for start in range(0, rows, CHUNK):
        both = dot(
            lower,
            jnp.concatenate([high[start : start + CHUNK], low[start : start + CHUNK]], axis=1),
        )
        piece = both[:, :width] + both[:, width:] + carry
        carry = piece[CHUNK - 1 : CHUNK]
        pieces.append(piece)
    return jnp.concatenate(pieces, axis=0)


def recurrence_kernel(
    ep, heads, direct, me_ref, q_ref, ff_ref, fb_ref, v_ref, lf_ref, lb_ref, extra_ref, *refs
):
    out_ref, reach_f_ref, reach_b_ref = refs[:3]
    message_refs = refs[3:-3]
    mix_ref, msg_f, msg_b = refs[-3:]
    rows = q_ref.shape[0]
    width = q_ref.shape[1] // heads
    tail = 16
    row = lax.broadcasted_iota(jnp.int32, (CHUNK, CHUNK), 0)
    col = lax.broadcasted_iota(jnp.int32, (CHUNK, CHUNK), 1)
    lower = jnp.where(row >= col, 1.0, 0.0).astype(BF16)
    tail_row = lax.broadcasted_iota(jnp.int32, (tail, width), 0)
    decays = [jnp.zeros((tail, width), F32), jnp.zeros((tail, width), F32)]
    for head in range(heads):
        lanes = slice(head * width, (head + 1) * width)
        q = q_ref[:, lanes].astype(F32)
        q = q / (1.0 + jnp.exp(-q))
        v = v_ref[:, lanes]
        extra = jnp.transpose(jnp.broadcast_to(extra_ref[head : head + 1, :], (width, rows)))
        kf, gf = gate_terms(ff_ref[:, lanes], lf_ref[:, lanes], extra)
        kb, gb = gate_terms(fb_ref[:, lanes], lb_ref[:, lanes], extra)
        b = running_sum(gf, lower)
        total_f = b[rows - 1 : rows]
        ahead = running_sum(gb, lower)
        total_b = ahead[rows - 1 : rows]
        c = total_b - ahead + gb

        half = rows // 2
        while half >= CHUNK:
            for first in range(0, rows, 2 * half):
                mid, last = first + half, first + 2 * half
                one, two = slice(first, mid), slice(mid, last)
                ref_f, ref_b = b[mid - 1 : mid], c[mid : mid + 1]
                mix_ref[two, one] = dot(
                    (q[two] * jnp.exp(b[two] - ref_f)).astype(BF16),
                    (kf[one] * jnp.exp(ref_f - b[one])).astype(BF16),
                    NT,
                ).astype(BF16)
                mix_ref[one, two] = dot(
                    (q[one] * jnp.exp(c[one] - ref_b)).astype(BF16),
                    (kb[two] * jnp.exp(ref_b - c[two])).astype(BF16),
                    NT,
                ).astype(BF16)
            half //= 2
        for start in range(0, rows, CHUNK):
            here = slice(start, start + CHUNK)
            qc, kfc, kbc, bc, cc = q[here], kf[here], kb[here], b[here], c[here]
            mid_f, mid_b = [], []
            for first in range(0, CHUNK, FINE):
                at = first + FINE // 2
                mid_f.append(jnp.broadcast_to(bc[at - 1 : at], (FINE, width)))
                mid_b.append(jnp.broadcast_to(cc[at : at + 1], (FINE, width)))
            df = bc - jnp.concatenate(mid_f, axis=0)
            db = cc - jnp.concatenate(mid_b, axis=0)
            near_f = dot((qc * jnp.exp(df)).astype(BF16), (kfc * jnp.exp(-df)).astype(BF16), NT)
            near_b = dot((qc * jnp.exp(db)).astype(BF16), (kbc * jnp.exp(-db)).astype(BF16), NT)
            scores = jnp.where(row >= col, near_f, 0.0) + jnp.where(row <= col, near_b, 0.0)
            half = FINE
            while half < CHUNK:
                q_side, k_side = [], []
                for first in range(0, CHUNK, 2 * half):
                    mid, last = first + half, first + 2 * half
                    one, two = slice(first, mid), slice(mid, last)
                    ref_f, ref_b = bc[mid - 1 : mid], cc[mid : mid + 1]
                    q_side.append(qc[one] * jnp.exp(cc[one] - ref_b))
                    q_side.append(qc[two] * jnp.exp(bc[two] - ref_f))
                    k_side.append(kfc[one] * jnp.exp(ref_f - bc[one]))
                    k_side.append(kbc[two] * jnp.exp(ref_b - cc[two]))
                far = dot(
                    jnp.concatenate(q_side, axis=0).astype(BF16),
                    jnp.concatenate(k_side, axis=0).astype(BF16),
                    NT,
                )
                scores = jnp.where(row // half == col // half, scores, far)
                half *= 2
            mix_ref[here, here] = scores.astype(BF16)
        out_ref[:, lanes] = dot(mix_ref[...], v)
        reach_f_ref[:, lanes] = (q * jnp.exp(b)).astype(BF16)
        reach_b_ref[:, lanes] = (q * jnp.exp(c)).astype(BF16)
        for which, message, key, run, total in (
            (0, msg_f, kf, b, total_f),
            (1, msg_b, kb, c, total_b),
        ):
            state = dot(v, (key * jnp.exp(total - run)).astype(BF16), TN)
            message[lanes, :] = state.astype(BF16)
            high = total.astype(BF16).astype(F32)
            decays[which] = jnp.where(tail_row == head, high, decays[which])
            decays[which] = jnp.where(tail_row == heads + head, total - high, decays[which])
    edge = heads * width
    msg_f[edge : edge + tail, :] = decays[0].astype(BF16)
    msg_b[edge : edge + tail, :] = decays[1].astype(BF16)
    me = me_ref[0]
    for step in range(1, ep):
        if direct:
            later = (me ^ step) > me
            target = message_refs[step - 1]

            @pl.when(later)
            def _(target=target):
                target[...] = msg_f[...]

            @pl.when(jnp.logical_not(later))
            def _(target=target):
                target[...] = msg_b[...]
    if not direct:

        def fill(place, carry):
            message_refs[0][place] = jnp.where(place > me, msg_f[...], msg_b[...])
            return carry

        lax.fori_loop(0, ep, fill, 0)


def finish_kernel(
    ep, tp, heads, direct, me_ref, quarter_ref, out_ref, reach_f_ref, reach_b_ref, gate_ref, gain_ref, w_ref, *refs
):
    count = ep - 1 if direct else 1
    arrived = refs[:count]
    pieces = refs[count : count + tp]
    hidden_ref, in_f, in_b = refs[count + tp : count + tp + 3]
    rows = out_ref.shape[0]
    width = out_ref.shape[1] // heads
    edge = heads * width
    me, quarter = me_ref[0], quarter_ref[0]
    in_f[...] = jnp.zeros_like(in_f)
    in_b[...] = jnp.zeros_like(in_b)

    def join(state_ref, read):
        decay = read(slice(edge, edge + 16)).astype(F32)
        for head in range(heads):
            lanes = slice(head * width, (head + 1) * width)
            total = decay[head : head + 1] + decay[heads + head : heads + head + 1]
            state_ref[lanes, :] = state_ref[lanes, :] * jnp.exp(total) + read(lanes).astype(F32)

    if direct:
        held_ref = refs[-1]
        for step in range(1, ep):
            held_ref[me ^ step] = arrived[step - 1][...]
    else:
        held_ref = arrived[0]

    def forward(place, carry):
        join(in_f, lambda part: held_ref[place, part, :])
        return carry

    def backward(place, carry):
        join(in_b, lambda part: held_ref[ep - 1 - place, part, :])
        return carry

    lax.fori_loop(0, me, forward, 0)
    lax.fori_loop(0, ep - 1 - me, backward, 0)
    for head in range(heads):
        lanes = slice(head * width, (head + 1) * width)
        combined = (
            out_ref[:, lanes]
            + dot(reach_f_ref[:, lanes], in_f[lanes, :].astype(BF16), NT)
            + dot(reach_b_ref[:, lanes], in_b[lanes, :].astype(BF16), NT)
        )
        square = jnp.mean(combined * combined, axis=-1, keepdims=True)
        gate = gate_ref[:, lanes].astype(F32)
        gate = gate / (1.0 + jnp.exp(-gate))
        scaled = combined * lax.rsqrt(square + EPS) * gain_ref[:, lanes]
        hidden_ref[:, lanes] = (scaled * gate).astype(BF16)
    block = rows // tp
    for piece in range(tp):
        start = pl.multiple_of((quarter ^ piece) * block, block)
        part = hidden_ref[pl.ds(start, block), :]
        pieces[piece][...] = dot(part, w_ref[...]).astype(BF16)


def swap(array, axis, bit):
    size = lax.axis_size(axis)
    return lax.ppermute(array, axis, [(place, place ^ bit) for place in range(size)])


def gather_quarters(own, axis):
    size = lax.axis_size(axis)
    pieces = {0: own}
    bit = size // 2
    while bit:
        for held in list(pieces):
            pieces[held | bit] = swap(pieces[held], axis, bit)
        bit //= 2
    return [pieces[place] for place in range(size)]


def scatter_sum(pieces, axis):
    size = lax.axis_size(axis)
    sums = {place: piece for place, piece in enumerate(pieces)}
    bit = 1
    while bit < size:
        going = [place for place in sums if place & bit]
        arrived = [swap(sums[place].astype(BF16), axis, bit) for place in going]
        for place, piece in zip(going, arrived):
            del sums[place]
            sums[place ^ bit] = sums[place ^ bit].astype(F32) + piece.astype(F32)
        bit *= 2
    return sums[0].astype(BF16)


def routing_kernel(groups, experts, me_ref, quarter_ref, rows_ref, gain_ref, routes_ref, *outs):
    count, _ = rows_ref.shape
    slots = 2 * TOPK * count // experts
    per_group = experts * slots // groups
    wide = rows_ref[...].astype(F32)
    square = jnp.mean(wide * wide, axis=-1, keepdims=True)
    normed = (wide * lax.rsqrt(square + EPS) * gain_ref[...]).astype(BF16)
    row = lax.broadcasted_iota(jnp.int32, (count, count), 0)
    col = lax.broadcasted_iota(jnp.int32, (count, count), 1)
    before = jnp.where(row < col, 1.0, 0.0).astype(BF16)
    expert = lax.broadcasted_iota(jnp.int32, (experts, count), 0)
    member = routes_ref[0:1, :] == expert
    for k in range(1, TOPK):
        member = jnp.logical_or(member, routes_ref[k : k + 1, :] == expert)
    rank = dot(jnp.where(member, 1.0, 0.0).astype(BF16), before)
    rank = jnp.where(member, rank, -1.0).astype(BF16)
    for group, out_ref in enumerate(outs):
        slot = group * per_group + lax.broadcasted_iota(jnp.int32, (per_group, experts), 0)
        which = lax.broadcasted_iota(jnp.int32, (per_group, experts), 1)
        owner = slot // slots
        if groups > 1:
            owner = owner ^ me_ref[0]
        ranks = dot(jnp.where(owner == which, 1.0, 0.0).astype(BF16), rank)
        place = lax.broadcasted_iota(jnp.int32, (per_group, count), 0) % slots
        pick = jnp.where(ranks == place.astype(F32), 1.0, 0.0).astype(BF16)
        out_ref[...] = dot(pick, normed).astype(BF16)


def hidden_kernel(groups, parts, *refs):
    xs = refs[:groups]
    gates = refs[groups : groups + parts]
    ups = refs[groups + parts : groups + 2 * parts]
    out_ref = refs[groups + 2 * parts]
    x_buf, g_buf, u_buf, x_sem, g_sem, u_sem = refs[groups + 2 * parts + 1 :]
    rows = xs[0].shape[0]
    width = gates[0].shape[1]

    def x_copy(i):
        return pltpu.make_async_copy(xs[i], x_buf.at[pl.ds(i * rows, rows)], x_sem.at[i])

    def w_copy(i):
        return (
            pltpu.make_async_copy(gates[i], g_buf.at[i], g_sem.at[i]),
            pltpu.make_async_copy(ups[i], u_buf.at[i], u_sem.at[i]),
        )

    for i in range(groups):
        x_copy(i).start()
    for i in range(parts):
        for one in w_copy(i):
            one.start()
    for i in range(groups):
        x_copy(i).wait()
    for i in range(parts):
        for one in w_copy(i):
            one.wait()
        gated = dot(x_buf[...], g_buf[i])
        lifted = dot(x_buf[...], u_buf[i])
        opened = gated / (1.0 + jnp.exp(-gated))
        out_ref[:, i * width : (i + 1) * width] = (opened * lifted).astype(BF16)


def down_kernel(groups, parts, hidden_ref, *refs):
    outs = refs[-groups:]
    downs = refs[:-groups]
    rows = outs[0].shape[0]
    depth, width = downs[0].shape
    for chunk in range(len(downs) // parts):
        total = None
        for i in range(parts):
            term = dot(hidden_ref[:, i * depth : (i + 1) * depth], downs[chunk * parts + i][...])
            total = term if total is None else total + term
        for group, out_ref in enumerate(outs):
            out_ref[:, chunk * width : (chunk + 1) * width] = total[
                group * rows : (group + 1) * rows
            ].astype(BF16)


def blend_kernel(groups, experts, me_ref, quarter_ref, routes_ref, factor_ref, *refs):
    arrived = refs[:groups]
    out_ref = refs[-1]
    count = routes_ref.shape[1]
    slots = 2 * TOPK * count // experts
    row = lax.broadcasted_iota(jnp.int32, (count, count), 0)
    col = lax.broadcasted_iota(jnp.int32, (count, count), 1)
    before = jnp.where(row > col, 1.0, 0.0).astype(BF16)

    def column(line):
        return jnp.transpose(jnp.broadcast_to(line, (count, count)))

    named = [column(routes_ref[k : k + 1, :]) for k in range(TOPK)]
    hits = [named[k] == col for k in range(TOPK)]
    member = hits[0]
    for k in range(1, TOPK):
        member = jnp.logical_or(member, hits[k])
    rank = dot(before, jnp.where(member, 1.0, 0.0).astype(BF16))
    picks = []
    slot = lax.broadcasted_iota(jnp.int32, (count, experts * slots), 1)
    for k in range(TOPK):
        place = jnp.sum(jnp.where(hits[k], rank, 0.0), axis=1, keepdims=True).astype(jnp.int32)
        owner = named[k][:, :1]
        if groups > 1:
            owner = owner ^ me_ref[0]
        picks.append(jnp.where(slot == owner * slots + place, 1.0, 0.0).astype(BF16))
    pick = jnp.concatenate(picks, axis=0)
    results = jnp.concatenate([one[...] for one in arrived], axis=0)
    chosen = dot(pick, results)
    total = None
    for k in range(TOPK):
        factor = column(factor_ref[k : k + 1, :])[:, :1]
        term = chosen[k * count : (k + 1) * count] * factor
        total = term if total is None else total + term
    width = total.shape[1]
    done = 0
    for earlier in refs[groups:-1]:
        out_ref[:, done : done + width] = earlier[...]
        done += width
    out_ref[:, done : done + width] = total.astype(BF16)


def call(kernel, operands, **options):
    return pl.pallas_call(kernel, compiler_params=params(), **options)(*operands)


def shards(
    queries,
    forget_forward_logits,
    forget_backward_logits,
    values,
    output_gate_logits,
    lower_bound_forward,
    lower_bound_backward,
    extra_log_decay,
    head_norm_scale,
    output_projection,
    second_residual,
    expert_norm_scale,
    routes,
    specialist_mixing_factor,
    expert_gate_matrix,
    expert_up_matrix,
    expert_down_matrix,
):
    ep, tp = lax.axis_size("ep"), lax.axis_size("tp")
    direct = ep <= DIRECT_EP
    groups = ep if direct else 1
    me = lax.axis_index("ep").reshape(1).astype(jnp.int32)
    quarter = lax.axis_index("tp").reshape(1).astype(jnp.int32)
    rows_all, model = second_residual.shape
    count = rows_all // tp
    capacity = 2 * TOPK * count
    per_group = capacity // groups
    depth = expert_gate_matrix.shape[2]
    shape = jax.ShapeDtypeStruct
    routes_t = routes.T
    factor_t = specialist_mixing_factor.T
    half = ep // 2
    sets = {"far": list(range(half, ep)), "near": list(range(half))} if direct else {"all": [0]}

    gates = gather_quarters(expert_gate_matrix[0], "tp")
    ups = gather_quarters(expert_up_matrix[0], "tp")
    part = model // DOWN_PARTS
    downs = [
        gather_quarters(expert_down_matrix[0, :, i * part : (i + 1) * part], "tp")
        for i in range(DOWN_PARTS)
    ]

    def whole(grid_index, a, b):
        return (0, 0)

    outgoing = call(
        functools.partial(routing_kernel, groups, ep),
        (me, quarter, second_residual, expert_norm_scale.reshape(1, -1), routes_t),
        grid_spec=pltpu.PrefetchScalarGridSpec(
            num_scalar_prefetch=2,
            grid=(1,),
            in_specs=[
                pl.BlockSpec((count, model), lambda i, a, b: (b[0], 0)),
                pl.BlockSpec((1, model), whole),
                pl.BlockSpec((TOPK, count), lambda i, a, b: (0, b[0])),
            ],
            out_specs=[pl.BlockSpec((per_group, model), whole)] * groups,
        ),
        out_shape=[shape((per_group, model), BF16)] * groups,
        cost_estimate=cost(2 * capacity * count * model, 2 * (count + capacity) * model),
    )

    def exchange(blocks):
        if direct:
            return {
                step: swap(block, "ep", step) if step else block
                for step, block in blocks.items()
            }
        stacked = blocks[0].reshape(ep, capacity // ep, -1)
        moved = lax.all_to_all(stacked, "ep", split_axis=0, concat_axis=0, tiled=True)
        return {0: moved.reshape(capacity, -1)}

    arrived = {}
    for chosen in sets.values():
        arrived.update(exchange({step: outgoing[step] for step in chosen}))

    rows, key_width = queries.shape
    heads = extra_log_decay.shape[1]
    message = (key_width + 16, key_width // heads)
    if direct:
        message_shapes = [shape(message, BF16)] * (ep - 1)
    else:
        message_shapes = [shape((ep,) + message, BF16)]
    local = call(
        functools.partial(recurrence_kernel, ep, heads, direct),
        (
            me,
            queries,
            forget_forward_logits,
            forget_backward_logits,
            values,
            lower_bound_forward.reshape(1, -1),
            lower_bound_backward.reshape(1, -1),
            extra_log_decay.T,
        ),
        in_specs=[SM] + [VM] * 7,
        out_specs=[VM] * (3 + len(message_shapes)),
        out_shape=[
            shape((rows, key_width), F32),
            shape((rows, key_width), BF16),
            shape((rows, key_width), BF16),
        ]
        + message_shapes,
        scratch_shapes=[
            pltpu.VMEM((rows, rows), BF16),
            pltpu.VMEM(message, BF16),
            pltpu.VMEM(message, BF16),
        ],
        cost_estimate=cost(12e9, 8 * rows * key_width, 20 * rows * key_width),
    )
    inner, reach_f, reach_b = local[:3]
    if direct:
        states = [swap(local[2 + step], "ep", step) for step in range(1, ep)]
    else:
        states = [lax.all_to_all(local[3], "ep", split_axis=0, concat_axis=0, tiled=True)]

    returned = [{} for _ in range(DOWN_PARTS)]
    for name, chosen in sets.items():
        size = len(chosen) * per_group
        hidden = call(
            functools.partial(hidden_kernel, len(chosen), tp),
            [arrived[step] for step in chosen] + gates + ups,
            in_specs=[HBM] * (len(chosen) + 2 * tp),
            out_specs=VM,
            out_shape=shape((size, tp * depth), BF16),
            scratch_shapes=[
                pltpu.VMEM((size, model), BF16),
                pltpu.VMEM((tp, model, depth), BF16),
                pltpu.VMEM((tp, model, depth), BF16),
                pltpu.SemaphoreType.DMA((len(chosen),)),
                pltpu.SemaphoreType.DMA((tp,)),
                pltpu.SemaphoreType.DMA((tp,)),
            ],
            cost_estimate=cost(4 * size * model * tp * depth, 4 * model * tp * depth),
        )
        batches = [list(range(DOWN_PARTS))] if name == "near" else [[i] for i in range(DOWN_PARTS)]
        for batch in batches:
            wide = part * len(batch)
            results = call(
                functools.partial(down_kernel, len(chosen), tp),
                [hidden] + [piece for i in batch for piece in downs[i]],
                in_specs=[VM] * (1 + tp * len(batch)),
                out_specs=[VM] * len(chosen),
                out_shape=[shape((per_group, wide), BF16)] * len(chosen),
                cost_estimate=cost(2 * size * tp * depth * wide, 2 * tp * depth * wide),
            )
            back = exchange(dict(zip(chosen, results)))
            for at, i in enumerate(batch):
                returned[i].update({step: (block, at) for step, block in back.items()})

    mixed = call(
        functools.partial(finish_kernel, ep, tp, heads, direct),
        (
            me,
            quarter,
            inner,
            reach_f,
            reach_b,
            output_gate_logits,
            head_norm_scale.reshape(1, -1),
            output_projection,
            *states,
        ),
        in_specs=[SM, SM] + [VM] * (6 + len(states)),
        out_specs=[VM] * tp,
        out_shape=[shape((rows // tp, model), BF16)] * tp,
        scratch_shapes=[
            pltpu.VMEM((rows, key_width), BF16),
            pltpu.VMEM((key_width, key_width // heads), F32),
            pltpu.VMEM((key_width, key_width // heads), F32),
        ]
        + ([pltpu.VMEM((ep,) + message, BF16)] if direct else []),
        cost_estimate=cost(2 * rows * key_width * model, 6 * rows * model, rows * key_width),
    )
    mixer_output = scatter_sum(mixed, "tp")

    ready = []
    for i in range(DOWN_PARTS):
        last = i == DOWN_PARTS - 1
        width = model if last else part
        blocks = [returned[i][step] for step in range(groups)]
        ready.append(
            call(
                functools.partial(blend_kernel, groups, ep),
                (
                    me,
                    quarter,
                    routes_t,
                    factor_t,
                    *[block for block, at in blocks],
                    *(ready if last else []),
                ),
                grid_spec=pltpu.PrefetchScalarGridSpec(
                    num_scalar_prefetch=2,
                    grid=(1,),
                    in_specs=[
                        pl.BlockSpec((TOPK, count), lambda i, a, b: (0, b[0])),
                        pl.BlockSpec((TOPK, count), whole),
                    ]
                    + [
                        pl.BlockSpec((per_group, part), lambda i, a, b, at=at: (0, at))
                        for block, at in blocks
                    ]
                    + [pl.BlockSpec((count, part), whole)] * (i if last else 0),
                    out_specs=pl.BlockSpec((count, width), whole),
                ),
                out_shape=shape((count, width), BF16),
                cost_estimate=cost(2 * TOPK * count * capacity * part, 2 * capacity * part),
            )
        )
    return (mixer_output, ready[-1])


def solution(mesh):
    in_specs = (
        P("ep", "tp"),
        P("ep", "tp"),
        P("ep", "tp"),
        P("ep", "tp"),
        P("ep", "tp"),
        P("tp"),
        P("tp"),
        P("ep", "tp"),
        P("tp"),
        P("tp", None),
        P("ep", None),
        P(),
        P("ep", None),
        P(("ep", "tp"), None),
        P("ep", None, "tp"),
        P("ep", None, "tp"),
        P("ep", "tp", None),
    )
    out_specs = (P(("ep", "tp"), None), P(("ep", "tp"), None))
    return jax.shard_map(shards, mesh=mesh, in_specs=in_specs, out_specs=out_specs, check_vma=False)
```

profile of v0, /device:TPU:0, one launch (start us, length us, event | category | flops | bytes accessed | tf_op | source)
XLA Modules:
  0.0 191.7 jit_solution(12158961502577195010)
XLA Ops:
  0.6 5.6 %shard_map.176 = (f32[512,256]{1,0:T(8,128)}, bf16[512,256]{1,0:T(8,128)(2,1)}, bf16[512,256]{1,0:T(8,128)(2,1)}, bf16[272,128]{1,0:T(8,128)(2,1)}, bf16[272,128...) custom-call(s32[1]{0:T(128)} %bitcast.me_ref, ...), custom_call_target="tpu_custom_call" | custom-call | flops 12000000000 | bytes 1048576 | tf_op jit(solution)/shard_map/pallas_call | solution.py:385
  6.2 3.0 %collective-permute-start = (bf16[272,128]{1,0:T(8,128)(2,1)}, bf16[272,128]{1,0:T(8,128)(2,1)S(1)}, u32[]{:S(2)}, u32[]{:S(2)}) collective-permute-start(bf16[272,128]{1,0:T(8,128)(2,1)} %get-tuple-element.39), channel_id=1, source_target_pairs={{0,4},{4,0},{8,12},{12,8},{16,20},{20,16},{24,28},{28,24},{1,5},{5... | collective-permute-start | bytes 208904 | tf_op jit(solution)/shard_map/ppermute | solution.py:236
  9.3 3.7 %shard_map.178 = (bf16[64,2048]{1,0:T(8,128)(2,1)}, bf16[64,2048]{1,0:T(8,128)(2,1)}, bf16[64,2048]{1,0:T(8,128)(2,1)}, bf16[64,2048]{1,0:T(8,128)(2,1)}, bf16[6...) custom-call(s32[1]{0:T(128)} %bitcast.me_ref, ...), custom_call_target="tpu_custom_call" | custom-call | flops 268435456 | bytes 2621440 | tf_op jit(solution)/shard_map/pallas_call | solution.py:385
  15.1 2.6 %collective-permute-start.28 = (bf16[64,2048]{1,0:T(8,128)(2,1)}, bf16[64,2048]{1,0:T(8,128)(2,1)S(1)}, u32[]{:S(2)}, u32[]{:S(2)}) collective-permute-start(bf16[64,2048]{1,0:T(8,128)(2,1)} %get-tuple-element.58), channel_id=1, source_target_pairs={{0,16},{4,20},{8,24},{12,28},{16,0},{20,4},{24,8},{28,12},{1,17},{... | collective-permute-start | bytes 786440 | tf_op jit(solution)/shard_map/ppermute | solution.py:236
  18.1 2.5 %collective-permute-start.2 = (bf16[272,128]{1,0:T(8,128)(2,1)}, bf16[272,128]{1,0:T(8,128)(2,1)S(1)}, u32[]{:S(2)}, u32[]{:S(2)}) collective-permute-start(bf16[272,128]{1,0:T(8,128)(2,1)} %get-tuple-element.41), channel_id=1, source_target_pairs={{0,12},{4,8},{8,4},{12,0},{16,28},{20,24},{24,20},{28,16},{1,13},{... | collective-permute-start | bytes 208904 | tf_op jit(solution)/shard_map/ppermute | solution.py:236
  20.6 8.4 %collective-permute-done.1.refs_1_ = bf16[272,128]{1,0:T(8,128)(2,1)S(1)} collective-permute-done((bf16[272,128]{1,0:T(8,128)(2,1)}, bf16[272,128]{1,0:T(8,128)(2,1)S(1)}, u32[]{:S(2)}, u32[]{:S(2)}) %collective-permute-start.1) | collective-permute-done | bytes 69664 | tf_op jit(solution)/shard_map/ppermute | solution.py:236
  29.0 2.8 %collective-permute-start.3 = (bf16[272,128]{1,0:T(8,128)(2,1)}, bf16[272,128]{1,0:T(8,128)(2,1)S(1)}, u32[]{:S(2)}, u32[]{:S(2)}) collective-permute-start(bf16[272,128]{1,0:T(8,128)(2,1)} %get-tuple-element.42), channel_id=1, source_target_pairs={{0,16},{4,20},{8,24},{12,28},{16,0},{20,4},{24,8},{28,12},{1,17},{... | collective-permute-start | bytes 208904 | tf_op jit(solution)/shard_map/ppermute | solution.py:236
  33.7 3.7 %collective-permute-done.3.refs_3_ = bf16[272,128]{1,0:T(8,128)(2,1)S(1)} collective-permute-done((bf16[272,128]{1,0:T(8,128)(2,1)}, bf16[272,128]{1,0:T(8,128)(2,1)S(1)}, u32[]{:S(2)}, u32[]{:S(2)}) %collective-permute-start.3) | collective-permute-done | bytes 69664 | tf_op jit(solution)/shard_map/ppermute | solution.py:236
  37.4 3.7 %collective-permute-start.5 = (bf16[272,128]{1,0:T(8,128)(2,1)}, bf16[272,128]{1,0:T(8,128)(2,1)S(1)}, u32[]{:S(2)}, u32[]{:S(2)}) collective-permute-start(bf16[272,128]{1,0:T(8,128)(2,1)} %get-tuple-element.44), channel_id=1, source_target_pairs={{0,24},{4,28},{8,16},{12,20},{16,8},{20,12},{24,0},{28,4},{1,25},{... | collective-permute-start | bytes 208904 | tf_op jit(solution)/shard_map/ppermute | solution.py:236
  41.2 2.4 %collective-permute-start.6 = (bf16[272,128]{1,0:T(8,128)(2,1)}, bf16[272,128]{1,0:T(8,128)(2,1)S(1)}, u32[]{:S(2)}, u32[]{:S(2)}) collective-permute-start(bf16[272,128]{1,0:T(8,128)(2,1)} %get-tuple-element.45), channel_id=1, source_target_pairs={{0,28},{4,24},{8,20},{12,16},{16,12},{20,8},{24,4},{28,0},{1,29},{... | collective-permute-start | bytes 208904 | tf_op jit(solution)/shard_map/ppermute | solution.py:236
  45.5 3.0 %collective-permute-done.6.refs_6_ = bf16[272,128]{1,0:T(8,128)(2,1)S(1)} collective-permute-done((bf16[272,128]{1,0:T(8,128)(2,1)}, bf16[272,128]{1,0:T(8,128)(2,1)S(1)}, u32[]{:S(2)}, u32[]{:S(2)}) %collective-permute-start.6) | collective-permute-done | bytes 69664 | tf_op jit(solution)/shard_map/ppermute | solution.py:236
  50.8 2.4 %collective-permute-start.30 = (bf16[64,2048]{1,0:T(8,128)(2,1)}, bf16[64,2048]{1,0:T(8,128)(2,1)S(1)}, u32[]{:S(2)}, u32[]{:S(2)}) collective-permute-start(bf16[64,2048]{1,0:T(8,128)(2,1)} %get-tuple-element.60), channel_id=1, source_target_pairs={{0,24},{4,28},{8,16},{12,20},{16,8},{20,12},{24,0},{28,4},{1,25},{... | collective-permute-start | bytes 786440 | tf_op jit(solution)/shard_map/ppermute | solution.py:236
  53.9 2.3 %collective-permute-start.31 = (bf16[64,2048]{1,0:T(8,128)(2,1)}, bf16[64,2048]{1,0:T(8,128)(2,1)S(1)}, u32[]{:S(2)}, u32[]{:S(2)}) collective-permute-start(bf16[64,2048]{1,0:T(8,128)(2,1)} %get-tuple-element.61), channel_id=1, source_target_pairs={{0,28},{4,24},{8,20},{12,16},{16,12},{20,8},{24,4},{28,0},{1,29},{... | collective-permute-start | bytes 786440 | tf_op jit(solution)/shard_map/ppermute | solution.py:236
  56.2 14.7 %collective-permute-done.29.refs_1_ = bf16[64,2048]{1,0:T(8,128)(2,1)S(1)} collective-permute-done((bf16[64,2048]{1,0:T(8,128)(2,1)}, bf16[64,2048]{1,0:T(8,128)(2,1)S(1)}, u32[]{:S(2)}, u32[]{:S(2)}) %collective-permute-start.29) | collective-permute-done | bytes 262176 | tf_op jit(solution)/shard_map/ppermute | solution.py:236
  73.8 4.3 %shard_map.177 = (bf16[128,2048]{1,0:T(8,128)(2,1)}, bf16[128,2048]{1,0:T(8,128)(2,1)}, bf16[128,2048]{1,0:T(8,128)(2,1)}, bf16[128,2048]{1,0:T(8,128)(2,1)}) custom-call(s32[1]{0:T(128)} %bitcast.me_ref, s32[1]{0:T(128)} %bitcast.1.quarter_ref, f32[512,256]{1,0:T(8,128)} %get-tuple-element.36.out_ref, bf16[512,256]{1,0:T(8,128)(2,1)} %get-tuple-element.37.reach_f_ref, ...), custom_call_target="tpu_custom_call" | custom-call | flops 536870912 | bytes 6291456 | tf_op jit(solution)/shard_map/pallas_call | solution.py:385
  78.1 26.1 %collective-permute-done.20.refs_2_ = bf16[256,1024]{1,0:T(8,128)(2,1)} collective-permute-done((bf16[256,1024]{1,0:T(8,128)(2,1)S(1)}, bf16[256,1024]{1,0:T(8,128)(2,1)}, u32[]{:S(2)}, u32[]{:S(2)}) %collective-permute-start.20) | collective-permute-done | bytes 524320 | tf_op jit(solution)/shard_map/ppermute | solution.py:236
  104.1 5.6 %collective-permute-done.23.refs_6_.refs_2_ = bf16[256,1024]{1,0:T(8,128)(2,1)S(1)} collective-permute-done((bf16[256,1024]{1,0:T(8,128)(2,1)S(1)}, bf16[256,1024]{1,0:T(8,128)(2,1)S(1)}, u32[]{:S(2)}, u32[]{:S(2)}) %collective-permute-start.23) | collective-permute-done | bytes 524320 | tf_op jit(solution)/shard_map/ppermute | solution.py:236
  110.8 2.4 %collective-permute-done.8 = bf16[128,2048]{1,0:T(8,128)(2,1)S(1)} collective-permute-done((bf16[128,2048]{1,0:T(8,128)(2,1)}, bf16[128,2048]{1,0:T(8,128)(2,1)S(1)}, u32[]{:S(2)}, u32[]{:S(2)}) %collective-permute-start.8) | collective-permute-done | bytes 524320 | tf_op jit(solution)/shard_map/ppermute | solution.py:236
  114.1 3.0 %collective-permute-done.21.refs_3_ = bf16[256,1024]{1,0:T(8,128)(2,1)} collective-permute-done((bf16[256,1024]{1,0:T(8,128)(2,1)}, bf16[256,1024]{1,0:T(8,128)(2,1)}, u32[]{:S(2)}, u32[]{:S(2)}) %collective-permute-start.21) | collective-permute-done | bytes 524320 | tf_op jit(solution)/shard_map/ppermute | solution.py:236
  121.9 6.9 %shard_map.181.hidden_ref = bf16[256,1024]{1,0:T(8,128)(2,1)} custom-call(bf16[64,2048]{1,0:T(8,128)(2,1)} %copy-done.20, bf16[64,2048]{1,0:T(8,128)(2,1)} %copy-done.21, bf16[64,2048]{1,0:T(8,128)(2,1)} %copy-done.22, bf16[64,2048]{1,0:T(8,128)(2,1)} %copy-done.23, bf16[2048,256]{1,0:T(8,128)(2,1)} %bitcast.15, bf16[2048,256]{1,0:T(8,128)(2,1)} %copy-done.6, ...), custom_call_target="tpu_custom_call" | custom-call | flops 2147483648 | bytes 8388608 | tf_op jit(solution)/shard_map/pallas_call | solution.py:385
  128.8 3.2 %shard_map.183 = (bf16[64,1024]{1,0:T(8,128)(2,1)}, bf16[64,1024]{1,0:T(8,128)(2,1)}, bf16[64,1024]{1,0:T(8,128)(2,1)}, bf16[64,1024]{1,0:T(8,128)(2,1)}) custom-call(bf16[256,1024]{1,0:T(8,128)(2,1)} %shard_map.181.hidden_ref, bf16[256,1024]{1,0:T(8,128)(2,1)} %copy-done.1, bf16[256,1024]{1,0:T(8,128)(2,1)} %collective-permute-done.19.refs_1_, ...), custom_call_target="tpu_custom_call" | custom-call | flops 536870912 | bytes 2097152 | tf_op jit(solution)/shard_map/pallas_call | solution.py:385
  133.5 6.9 %shard_map.179.hidden_ref = bf16[256,1024]{1,0:T(8,128)(2,1)} custom-call(bf16[64,2048]{1,0:T(8,128)(2,1)} %get-tuple-element.50.refs_0_, bf16[64,2048]{1,0:T(8,128)(2,1)} %copy-done.18, bf16[64,2048]{1,0:T(8,128)(2,1)} %copy-done.19, bf16[64,2048]{1,0:T(8,128)(2,1)} %copy-done.24, bf16[2048,256]{1,0:T(8,128)(2,1)} %bitcast.16, bf16[2048,256]{1,0:T(8,128)(2,1)} %copy-done.6, ...), custom_call_target="tpu_custom_call" | custom-call | flops 2147483648 | bytes 8388608 | tf_op jit(solution)/shard_map/pallas_call | solution.py:385
  142.0 4.5 %shard_map.180 = (bf16[64,2048]{1,0:T(8,128)(2,1)}, bf16[64,2048]{1,0:T(8,128)(2,1)}, bf16[64,2048]{1,0:T(8,128)(2,1)}, bf16[64,2048]{1,0:T(8,128)(2,1)}) custom-call(bf16[256,1024]{1,0:T(8,128)(2,1)} %shard_map.179.hidden_ref, bf16[256,1024]{1,0:T(8,128)(2,1)} %copy-done.1, bf16[256,1024]{1,0:T(8,128)(2,1)} %collective-permute-done.19.refs_1_, ...), custom_call_target="tpu_custom_call" | custom-call | flops 1073741824 | bytes 4194304 | tf_op jit(solution)/shard_map/pallas_call | solution.py:385
  149.7 2.7 %collective-permute-start.38 = (bf16[64,1024]{1,0:T(8,128)(2,1)S(1)}, bf16[64,1024]{1,0:T(8,128)(2,1)S(1)}, u32[]{:S(2)}, u32[]{:S(2)}) collective-permute-start(bf16[64,1024]{1,0:T(8,128)(2,1)S(1)} %copy-done.42), channel_id=1, source_target_pairs={{0,24},{4,28},{8,16},{12,20},{16,8},{20,12},{24,0},{28,4},{1,25},{... | collective-permute-start | bytes 393224 | tf_op jit(solution)/shard_map/ppermute | solution.py:236
  153.8 3.1 %shard_map.182 = (bf16[64,1024]{1,0:T(8,128)(2,1)}, bf16[64,1024]{1,0:T(8,128)(2,1)}, bf16[64,1024]{1,0:T(8,128)(2,1)}, bf16[64,1024]{1,0:T(8,128)(2,1)}) custom-call(bf16[256,1024]{1,0:T(8,128)(2,1)} %shard_map.181.hidden_ref, bf16[256,1024]{1,0:T(8,128)(2,1)} %copy-done, bf16[256,1024]{1,0:T(8,128)(2,1)} %copy-done.11, bf16[256,1024]{1,0:T(8,128)(2,1)} %copy-done.10, ...), custom_call_target="tpu_custom_call" | custom-call | flops 536870912 | bytes 2097152 | tf_op jit(solution)/shard_map/pallas_call | solution.py:385
  157.9 4.2 %collective-permute-start.27 = (bf16[64,2048]{1,0:T(8,128)(2,1)S(1)}, bf16[64,2048]{1,0:T(8,128)(2,1)S(1)}, u32[]{:S(2)}, u32[]{:S(2)}) collective-permute-start(bf16[64,2048]{1,0:T(8,128)(2,1)S(1)} %copy-done.40), channel_id=1, source_target_pairs={{0,12},{4,8},{8,4},{12,0},{16,28},{20,24},{24,20},{28,16},{1,13},{... | collective-permute-start | bytes 786440 | tf_op jit(solution)/shard_map/ppermute | solution.py:236
  163.5 5.2 %collective-permute-start.32 = (bf16[64,1024]{1,0:T(8,128)(2,1)}, bf16[64,1024]{1,0:T(8,128)(2,1)S(1)}, u32[]{:S(2)}, u32[]{:S(2)}) collective-permute-start(bf16[64,1024]{1,0:T(8,128)(2,1)} %get-tuple-element.62), channel_id=1, source_target_pairs={{0,16},{4,20},{8,24},{12,28},{16,0},{20,4},{24,8},{28,12},{1,17},{... | collective-permute-start | bytes 393224 | tf_op jit(solution)/shard_map/ppermute | solution.py:236
  168.6 4.9 %collective-permute-start.33 = (bf16[64,1024]{1,0:T(8,128)(2,1)}, bf16[64,1024]{1,0:T(8,128)(2,1)S(1)}, u32[]{:S(2)}, u32[]{:S(2)}) collective-permute-start(bf16[64,1024]{1,0:T(8,128)(2,1)} %get-tuple-element.63), channel_id=1, source_target_pairs={{0,20},{4,16},{8,28},{12,24},{16,4},{20,0},{24,12},{28,8},{1,21},{... | collective-permute-start | bytes 393224 | tf_op jit(solution)/shard_map/ppermute | solution.py:236
  174.9 2.9 %collective-permute-start.35 = (bf16[64,1024]{1,0:T(8,128)(2,1)}, bf16[64,1024]{1,0:T(8,128)(2,1)S(1)}, u32[]{:S(2)}, u32[]{:S(2)}) collective-permute-start(bf16[64,1024]{1,0:T(8,128)(2,1)} %get-tuple-element.65), channel_id=1, source_target_pairs={{0,28},{4,24},{8,20},{12,16},{16,12},{20,8},{24,4},{28,0},{1,29},{... | collective-permute-start | bytes 393224 | tf_op jit(solution)/shard_map/ppermute | solution.py:236
  179.5 2.9 %shard_map.184.refs_8_ = bf16[128,1024]{1,0:T(8,128)(2,1)} custom-call(s32[1]{0:T(128)} %bitcast.me_ref, s32[1]{0:T(128)} %bitcast.1.quarter_ref, s32[2,512]{1,0:T(2,128)} %bitcast.24, f32[2,128]{1,0:T(2,128)} %bitcast.27, bf16[64,2048]{1,0:T(8,128)(2,1)} %get-tuple-element.54.refs_0_, bf16[64,2048]{1,0:T(8,128)(2,1)} %copy-done.14, ...), custom_call_target="tpu_custom_call" | custom-call | flops 268435456 | bytes 1048576 | tf_op jit(solution)/shard_map/pallas_call | solution.py:385
  183.6 3.5 %collective-permute-done.33.refs_5_ = bf16[64,1024]{1,0:T(8,128)(2,1)S(1)} collective-permute-done((bf16[64,1024]{1,0:T(8,128)(2,1)}, bf16[64,1024]{1,0:T(8,128)(2,1)S(1)}, u32[]{:S(2)}, u32[]{:S(2)}) %collective-permute-start.33) | collective-permute-done | bytes 131104 | tf_op jit(solution)/shard_map/ppermute | solution.py:236
  188.6 3.1 %shard_map.185 = bf16[128,2048]{1,0:T(8,128)(2,1)} custom-call(s32[1]{0:T(128)} %bitcast.me_ref, s32[1]{0:T(128)} %bitcast.1.quarter_ref, s32[2,512]{1,0:T(2,128)} %bitcast.25, f32[2,128]{1,0:T(2,128)} %bitcast.28, bf16[64,2048]{1,0:T(8,128)(2,1)} %get-tuple-element.54.refs_0_, bf16[64,2048]{1,0:T(8,128)(2,1)} %copy-done.14, bf16[64,2048]{1,0:T(8,128)(2,1)} %copy-done.15, ...), custom_call_target="tpu_custom_call" | custom-call | flops 268435456 | bytes 1048576 | tf_op jit(solution)/shard_map/pallas_call | solution.py:385
  (149 shorter events, 34.5 us)
Async XLA Ops:
  6.2 11.9 %collective-permute-start = (bf16[272,128]{1,0:T(8,128)(2,1)}, bf16[272,128]{1,0:T(8,128)(2,1)S(1)}, u32[]{:S(2)}, u32[]{:S(2)}) collective-permute-start(bf16[272,128]{1,0:T(8,128)(2,1)} %get-tuple-element.39), channel_id=1, source_target_pairs={{0,4},{4,0},{8,12},{12,8},{16,20},{20,16},{24,28},{28,24},{1,5},{5... | collective-permute-start | bytes 208904 | tf_op jit(solution)/shard_map/ppermute | solution.py:236
  13.0 37.8 %collective-permute-start.10 = (bf16[64,2048]{1,0:T(8,128)(2,1)}, bf16[64,2048]{1,0:T(8,128)(2,1)S(1)}, u32[]{:S(2)}, u32[]{:S(2)}) collective-permute-start(bf16[64,2048]{1,0:T(8,128)(2,1)} %get-tuple-element.51), channel_id=1, source_target_pairs={{0,4},{4,0},{8,12},{12,8},{16,20},{20,16},{24,28},{28,24},{1,5},{5... | collective-permute-start | bytes 786440 | tf_op jit(solution)/shard_map/ppermute | solution.py:236
  13.1 37.6 %collective-permute-start.11 = (bf16[64,2048]{1,0:T(8,128)(2,1)}, bf16[64,2048]{1,0:T(8,128)(2,1)S(1)}, u32[]{:S(2)}, u32[]{:S(2)}) collective-permute-start(bf16[64,2048]{1,0:T(8,128)(2,1)} %get-tuple-element.52), channel_id=1, source_target_pairs={{0,8},{4,12},{8,0},{12,4},{16,24},{20,28},{24,16},{28,20},{1,9},{5... | collective-permute-start | bytes 786440 | tf_op jit(solution)/shard_map/ppermute | solution.py:236
  15.1 38.0 %collective-permute-start.28 = (bf16[64,2048]{1,0:T(8,128)(2,1)}, bf16[64,2048]{1,0:T(8,128)(2,1)S(1)}, u32[]{:S(2)}, u32[]{:S(2)}) collective-permute-start(bf16[64,2048]{1,0:T(8,128)(2,1)} %get-tuple-element.58), channel_id=1, source_target_pairs={{0,16},{4,20},{8,24},{12,28},{16,0},{20,4},{24,8},{28,12},{1,17},{... | collective-permute-start | bytes 786440 | tf_op jit(solution)/shard_map/ppermute | solution.py:236
  17.7 11.3 %collective-permute-start.1 = (bf16[272,128]{1,0:T(8,128)(2,1)}, bf16[272,128]{1,0:T(8,128)(2,1)S(1)}, u32[]{:S(2)}, u32[]{:S(2)}) collective-permute-start(bf16[272,128]{1,0:T(8,128)(2,1)} %get-tuple-element.40), channel_id=1, source_target_pairs={{0,8},{4,12},{8,0},{12,4},{16,24},{20,28},{24,16},{28,20},{1,9},{5... | collective-permute-start | bytes 208904 | tf_op jit(solution)/shard_map/ppermute | solution.py:236
  18.1 13.7 %collective-permute-start.2 = (bf16[272,128]{1,0:T(8,128)(2,1)}, bf16[272,128]{1,0:T(8,128)(2,1)S(1)}, u32[]{:S(2)}, u32[]{:S(2)}) collective-permute-start(bf16[272,128]{1,0:T(8,128)(2,1)} %get-tuple-element.41), channel_id=1, source_target_pairs={{0,12},{4,8},{8,4},{12,0},{16,28},{20,24},{24,20},{28,16},{1,13},{... | collective-permute-start | bytes 208904 | tf_op jit(solution)/shard_map/ppermute | solution.py:236
  31.9 9.3 %collective-permute-start.4 = (bf16[272,128]{1,0:T(8,128)(2,1)}, bf16[272,128]{1,0:T(8,128)(2,1)S(1)}, u32[]{:S(2)}, u32[]{:S(2)}) collective-permute-start(bf16[272,128]{1,0:T(8,128)(2,1)} %get-tuple-element.43), channel_id=1, source_target_pairs={{0,20},{4,16},{8,28},{12,24},{16,4},{20,0},{24,12},{28,8},{1,21},{... | collective-permute-start | bytes 208904 | tf_op jit(solution)/shard_map/ppermute | solution.py:236
  44.3 66.0 %collective-permute-start.14 = (bf16[2048,256]{1,0:T(8,128)(2,1)S(1)}, bf16[2048,256]{1,0:T(8,128)(2,1)S(1)}, u32[]{:S(2)}, u32[]{:S(2)}) collective-permute-start(bf16[2048,256]{1,0:T(8,128)(2,1)S(1)} %bitcast.17), channel_id=1, source_target_pairs={{0,2},{1,3},{2,0},{3,1},{4,6},{5,7},{6,4},{7,5},{8,10},{9,11},{10,... | collective-permute-start | bytes 3145736 | tf_op jit(solution)/shard_map/ppermute | solution.py:236
  48.5 61.9 %collective-permute-start.17 = (bf16[2048,256]{1,0:T(8,128)(2,1)S(1)}, bf16[2048,256]{1,0:T(8,128)(2,1)S(1)}, u32[]{:S(2)}, u32[]{:S(2)}) collective-permute-start(bf16[2048,256]{1,0:T(8,128)(2,1)S(1)} %bitcast.21), channel_id=1, source_target_pairs={{0,2},{1,3},{2,0},{3,1},{4,6},{5,7},{6,4},{7,5},{8,10},{9,11},{10,... | collective-permute-start | bytes 3145736 | tf_op jit(solution)/shard_map/ppermute | solution.py:236
  50.8 20.2 %collective-permute-start.29 = (bf16[64,2048]{1,0:T(8,128)(2,1)}, bf16[64,2048]{1,0:T(8,128)(2,1)S(1)}, u32[]{:S(2)}, u32[]{:S(2)}) collective-permute-start(bf16[64,2048]{1,0:T(8,128)(2,1)} %get-tuple-element.59), channel_id=1, source_target_pairs={{0,20},{4,16},{8,28},{12,24},{16,4},{20,0},{24,12},{28,8},{1,21},{... | collective-permute-start | bytes 786440 | tf_op jit(solution)/shard_map/ppermute | solution.py:236
  50.8 21.5 %collective-permute-start.30 = (bf16[64,2048]{1,0:T(8,128)(2,1)}, bf16[64,2048]{1,0:T(8,128)(2,1)S(1)}, u32[]{:S(2)}, u32[]{:S(2)}) collective-permute-start(bf16[64,2048]{1,0:T(8,128)(2,1)} %get-tuple-element.60), channel_id=1, source_target_pairs={{0,24},{4,28},{8,16},{12,20},{16,8},{20,12},{24,0},{28,4},{1,25},{... | collective-permute-start | bytes 786440 | tf_op jit(solution)/shard_map/ppermute | solution.py:236
  53.9 19.8 %collective-permute-start.31 = (bf16[64,2048]{1,0:T(8,128)(2,1)}, bf16[64,2048]{1,0:T(8,128)(2,1)S(1)}, u32[]{:S(2)}, u32[]{:S(2)}) collective-permute-start(bf16[64,2048]{1,0:T(8,128)(2,1)} %get-tuple-element.61), channel_id=1, source_target_pairs={{0,28},{4,24},{8,20},{12,16},{16,12},{20,8},{24,4},{28,0},{1,29},{... | collective-permute-start | bytes 786440 | tf_op jit(solution)/shard_map/ppermute | solution.py:236
  70.9 33.2 %collective-permute-start.20 = (bf16[256,1024]{1,0:T(8,128)(2,1)S(1)}, bf16[256,1024]{1,0:T(8,128)(2,1)}, u32[]{:S(2)}, u32[]{:S(2)}) collective-permute-start(bf16[256,1024]{1,0:T(8,128)(2,1)S(1)} %get-tuple-element.71.refs_0_), channel_id=1, source_target_pairs={{0,2},{1,3},{2,0},{3,1},{4,6},{5,7},{6,4},{7,5},{8,10},{9,11},{10,... | collective-permute-start | bytes 1572872 | tf_op jit(solution)/shard_map/ppermute | solution.py:236
  72.9 36.8 %collective-permute-start.23 = (bf16[256,1024]{1,0:T(8,128)(2,1)S(1)}, bf16[256,1024]{1,0:T(8,128)(2,1)S(1)}, u32[]{:S(2)}, u32[]{:S(2)}) collective-permute-start(bf16[256,1024]{1,0:T(8,128)(2,1)S(1)} %get-tuple-element.70.refs_4_.refs_0_), channel_id=1, source_target_pairs={{0,2},{1,3},{2,0},{3,1},{4,6},{5,7},{6,4},{7,5},{8,10},{9,11},{10,... | collective-permute-start | bytes 1572872 | tf_op jit(solution)/shard_map/ppermute | solution.py:236
  73.7 36.1 %collective-permute-start.19 = (bf16[256,1024]{1,0:T(8,128)(2,1)S(1)}, bf16[256,1024]{1,0:T(8,128)(2,1)}, u32[]{:S(2)}, u32[]{:S(2)}) collective-permute-start(bf16[256,1024]{1,0:T(8,128)(2,1)S(1)} %get-tuple-element.71.refs_0_), channel_id=1, source_target_pairs={{0,1},{1,0},{2,3},{3,2},{4,5},{5,4},{6,7},{7,6},{8,9},{9,8},{10,11... | collective-permute-start | bytes 1572872 | tf_op jit(solution)/shard_map/ppermute | solution.py:236
  104.1 9.2 %collective-permute-start.13 = (bf16[2048,256]{1,0:T(8,128)(2,1)S(1)}, bf16[2048,256]{1,0:T(8,128)(2,1)S(1)}, u32[]{:S(2)}, u32[]{:S(2)}) collective-permute-start(bf16[2048,256]{1,0:T(8,128)(2,1)S(1)} %bitcast.18), channel_id=1, source_target_pairs={{0,1},{1,0},{2,3},{3,2},{4,5},{5,4},{6,7},{7,6},{8,9},{9,8},{10,11... | collective-permute-start | bytes 3145736 | tf_op jit(solution)/shard_map/ppermute | solution.py:236
  113.3 27.1 %collective-permute-start.22 = (bf16[256,1024]{1,0:T(8,128)(2,1)S(1)}, bf16[256,1024]{1,0:T(8,128)(2,1)S(1)}, u32[]{:S(2)}, u32[]{:S(2)}) collective-permute-start(bf16[256,1024]{1,0:T(8,128)(2,1)S(1)} %get-tuple-element.70.refs_4_.refs_0_), channel_id=1, source_target_pairs={{0,1},{1,0},{2,3},{3,2},{4,5},{5,4},{6,7},{7,6},{8,9},{9,8},{10,11... | collective-permute-start | bytes 1572872 | tf_op jit(solution)/shard_map/ppermute | solution.py:236
  113.7 18.3 %collective-permute-start.12 = (bf16[64,2048]{1,0:T(8,128)(2,1)}, bf16[64,2048]{1,0:T(8,128)(2,1)S(1)}, u32[]{:S(2)}, u32[]{:S(2)}) collective-permute-start(bf16[64,2048]{1,0:T(8,128)(2,1)} %get-tuple-element.53), channel_id=1, source_target_pairs={{0,12},{4,8},{8,4},{12,0},{16,28},{20,24},{24,20},{28,16},{1,13},{... | collective-permute-start | bytes 786440 | tf_op jit(solution)/shard_map/ppermute | solution.py:236
  117.1 23.3 %collective-permute-start.24 = (bf16[256,1024]{1,0:T(8,128)(2,1)S(1)}, bf16[256,1024]{1,0:T(8,128)(2,1)S(1)}, u32[]{:S(2)}, u32[]{:S(2)}) collective-permute-start(bf16[256,1024]{1,0:T(8,128)(2,1)S(1)} %collective-permute-done.23.refs_6_.refs_2_), channel_id=1, source_target_pairs={{0,1},{1,0},{2,3},{3,2},{4,5},{5,4},{6,7},{7,6},{8,9},{9,8},{10,11... | collective-permute-start | bytes 1572872 | tf_op jit(solution)/shard_map/ppermute | solution.py:236
  118.4 29.7 %collective-permute-start.7 = (bf16[128,2048]{1,0:T(8,128)(2,1)}, bf16[128,2048]{1,0:T(8,128)(2,1)S(1)}, u32[]{:S(2)}, u32[]{:S(2)}) collective-permute-start(bf16[128,2048]{1,0:T(8,128)(2,1)} %get-tuple-element.47), channel_id=1, source_target_pairs={{0,1},{1,0},{2,3},{3,2},{4,5},{5,4},{6,7},{7,6},{8,9},{9,8},{10,11... | collective-permute-start | bytes 1572872 | tf_op jit(solution)/shard_map/ppermute | solution.py:236
  120.3 29.3 %collective-permute-start.9 = (bf16[128,2048]{1,0:T(8,128)(2,1)S(1)}, bf16[128,2048]{1,0:T(8,128)(2,1)S(1)}, u32[]{:S(2)}, u32[]{:S(2)}) collective-permute-start(bf16[128,2048]{1,0:T(8,128)(2,1)S(1)} %add_convert_fusion.1), channel_id=1, source_target_pairs={{0,2},{1,3},{2,0},{3,1},{4,6},{5,7},{6,4},{7,5},{8,10},{9,11},{10,... | collective-permute-start | bytes 1572872 | tf_op jit(solution)/shard_map/ppermute | solution.py:236
  132.0 20.4 %collective-permute-start.36 = (bf16[64,1024]{1,0:T(8,128)(2,1)}, bf16[64,1024]{1,0:T(8,128)(2,1)S(1)}, u32[]{:S(2)}, u32[]{:S(2)}) collective-permute-start(bf16[64,1024]{1,0:T(8,128)(2,1)} %get-tuple-element.66), channel_id=1, source_target_pairs={{0,16},{4,20},{8,24},{12,28},{16,0},{20,4},{24,8},{28,12},{1,17},{... | collective-permute-start | bytes 393224 | tf_op jit(solution)/shard_map/ppermute | solution.py:236
  146.5 27.1 %collective-permute-start.25 = (bf16[64,2048]{1,0:T(8,128)(2,1)}, bf16[64,2048]{1,0:T(8,128)(2,1)S(1)}, u32[]{:S(2)}, u32[]{:S(2)}) collective-permute-start(bf16[64,2048]{1,0:T(8,128)(2,1)} %get-tuple-element.55), channel_id=1, source_target_pairs={{0,4},{4,0},{8,12},{12,8},{16,20},{20,16},{24,28},{28,24},{1,5},{5... | collective-permute-start | bytes 786440 | tf_op jit(solution)/shard_map/ppermute | solution.py:236
  147.3 27.6 %collective-permute-start.26 = (bf16[64,2048]{1,0:T(8,128)(2,1)}, bf16[64,2048]{1,0:T(8,128)(2,1)S(1)}, u32[]{:S(2)}, u32[]{:S(2)}) collective-permute-start(bf16[64,2048]{1,0:T(8,128)(2,1)} %get-tuple-element.56), channel_id=1, source_target_pairs={{0,8},{4,12},{8,0},{12,4},{16,24},{20,28},{24,16},{28,20},{1,9},{5... | collective-permute-start | bytes 786440 | tf_op jit(solution)/shard_map/ppermute | solution.py:236
  148.1 9.8 %collective-permute-start.37 = (bf16[64,1024]{1,0:T(8,128)(2,1)S(1)}, bf16[64,1024]{1,0:T(8,128)(2,1)S(1)}, u32[]{:S(2)}, u32[]{:S(2)}) collective-permute-start(bf16[64,1024]{1,0:T(8,128)(2,1)S(1)} %copy-done.43), channel_id=1, source_target_pairs={{0,20},{4,16},{8,28},{12,24},{16,4},{20,0},{24,12},{28,8},{1,21},{... | collective-permute-start | bytes 393224 | tf_op jit(solution)/shard_map/ppermute | solution.py:236
  149.7 13.8 %collective-permute-start.38 = (bf16[64,1024]{1,0:T(8,128)(2,1)S(1)}, bf16[64,1024]{1,0:T(8,128)(2,1)S(1)}, u32[]{:S(2)}, u32[]{:S(2)}) collective-permute-start(bf16[64,1024]{1,0:T(8,128)(2,1)S(1)} %copy-done.42), channel_id=1, source_target_pairs={{0,24},{4,28},{8,16},{12,20},{16,8},{20,12},{24,0},{28,4},{1,25},{... | collective-permute-start | bytes 393224 | tf_op jit(solution)/shard_map/ppermute | solution.py:236
  152.4 16.2 %collective-permute-start.39 = (bf16[64,1024]{1,0:T(8,128)(2,1)S(1)}, bf16[64,1024]{1,0:T(8,128)(2,1)S(1)}, u32[]{:S(2)}, u32[]{:S(2)}) collective-permute-start(bf16[64,1024]{1,0:T(8,128)(2,1)S(1)} %copy-done.41), channel_id=1, source_target_pairs={{0,28},{4,24},{8,20},{12,16},{16,12},{20,8},{24,4},{28,0},{1,29},{... | collective-permute-start | bytes 393224 | tf_op jit(solution)/shard_map/ppermute | solution.py:236
  157.9 20.9 %collective-permute-start.27 = (bf16[64,2048]{1,0:T(8,128)(2,1)S(1)}, bf16[64,2048]{1,0:T(8,128)(2,1)S(1)}, u32[]{:S(2)}, u32[]{:S(2)}) collective-permute-start(bf16[64,2048]{1,0:T(8,128)(2,1)S(1)} %copy-done.40), channel_id=1, source_target_pairs={{0,12},{4,8},{8,4},{12,0},{16,28},{20,24},{24,20},{28,16},{1,13},{... | collective-permute-start | bytes 786440 | tf_op jit(solution)/shard_map/ppermute | solution.py:236
  163.5 20.2 %collective-permute-start.32 = (bf16[64,1024]{1,0:T(8,128)(2,1)}, bf16[64,1024]{1,0:T(8,128)(2,1)S(1)}, u32[]{:S(2)}, u32[]{:S(2)}) collective-permute-start(bf16[64,1024]{1,0:T(8,128)(2,1)} %get-tuple-element.62), channel_id=1, source_target_pairs={{0,16},{4,20},{8,24},{12,28},{16,0},{20,4},{24,8},{28,12},{1,17},{... | collective-permute-start | bytes 393224 | tf_op jit(solution)/shard_map/ppermute | solution.py:236
  168.6 18.6 %collective-permute-start.33 = (bf16[64,1024]{1,0:T(8,128)(2,1)}, bf16[64,1024]{1,0:T(8,128)(2,1)S(1)}, u32[]{:S(2)}, u32[]{:S(2)}) collective-permute-start(bf16[64,1024]{1,0:T(8,128)(2,1)} %get-tuple-element.63), channel_id=1, source_target_pairs={{0,20},{4,16},{8,28},{12,24},{16,4},{20,0},{24,12},{28,8},{1,21},{... | collective-permute-start | bytes 393224 | tf_op jit(solution)/shard_map/ppermute | solution.py:236
  173.6 13.6 %collective-permute-start.34 = (bf16[64,1024]{1,0:T(8,128)(2,1)}, bf16[64,1024]{1,0:T(8,128)(2,1)S(1)}, u32[]{:S(2)}, u32[]{:S(2)}) collective-permute-start(bf16[64,1024]{1,0:T(8,128)(2,1)} %get-tuple-element.64), channel_id=1, source_target_pairs={{0,24},{4,28},{8,16},{12,20},{16,8},{20,12},{24,0},{28,4},{1,25},{... | collective-permute-start | bytes 393224 | tf_op jit(solution)/shard_map/ppermute | solution.py:236
  174.9 12.3 %collective-permute-start.35 = (bf16[64,1024]{1,0:T(8,128)(2,1)}, bf16[64,1024]{1,0:T(8,128)(2,1)S(1)}, u32[]{:S(2)}, u32[]{:S(2)}) collective-permute-start(bf16[64,1024]{1,0:T(8,128)(2,1)} %get-tuple-element.65), channel_id=1, source_target_pairs={{0,28},{4,24},{8,20},{12,16},{16,12},{20,8},{24,4},{28,0},{1,29},{... | collective-permute-start | bytes 393224 | tf_op jit(solution)/shard_map/ppermute | solution.py:236
  (52 other events, 836.9 us)
where the time goes:
time: 193 us; the launch traced here: 192 us
  waiting for transfers between devices  74.8 us (39%)
  starting transfers between devices  62.8 us (33%)
  Pallas kernels  44.2 us (23%)
  local copies, waits for them, and re-layouts  6.72 us (3%)
  other arithmetic  2.2 us (1%)
    ppermute x40, waiting for transfers between devices, swap(): lax.ppermute(array, axis, [(place, place ^ bit) for place in range(size)])  74.8 us
    ppermute x40, starting transfers between devices, swap(): lax.ppermute(array, axis, [(place, place ^ bit) for place in range(size)])  62.8 us
    pallas_call x10, Pallas kernels, call(): pl.pallas_call(kernel, compiler_params=params(), **options)(*operands)  44.2 us
    unnamed x88, local copies, waits for them, and re-layouts  6.64 us
  transfers between devices with their start and end apart: 40, of which 13 were waited for; matrix products, arithmetic and copies ran while one was open for 1% of the time, Pallas kernels for 19%

commit v1 on v0

v1 whole, which is shorter than its diff:
```python
import functools
import jax
import jax.numpy as jnp
from jax import lax
from jax.experimental import pallas as pl
from jax.experimental.pallas import tpu as pltpu
from jax.sharding import PartitionSpec as P

TOPK = 2
EPS = 1e-06
CHUNK = 128
FINE = 16
DIRECT_EP = 8
DOWN_EIGHTHS = (5, 3)
TILE = 256
F32 = jnp.float32
BF16 = jnp.bfloat16

NT = (((1,), (1,)), ((), ()))
TN = (((0,), (0,)), ((), ()))
VM = pl.BlockSpec(memory_space=pltpu.VMEM)
SM = pl.BlockSpec(memory_space=pltpu.SMEM)
HBM = pl.BlockSpec(memory_space=pl.ANY)


def cost(flops, moved, exps=0):
    return pl.CostEstimate(flops=int(flops), bytes_accessed=int(moved), transcendentals=int(exps))


def params(mebibytes):
    return pltpu.CompilerParams(vmem_limit_bytes=mebibytes * 1024 * 1024)


def dot(a, b, dims=(((1,), (0,)), ((), ()))):
    return lax.dot_general(a, b, dims, preferred_element_type=F32)


def gate_terms(logits, bound, extra):
    wide = logits.astype(F32)
    grown = jnp.exp(-wide)
    opened = 1.0 / (1.0 + grown)
    floor = jax.nn.sigmoid(bound)
    rest = jax.nn.sigmoid(-bound)
    return rest * (grown * opened), jnp.log(floor + rest * opened) + extra


def running_sum(decay, lower):
    rows, width = decay.shape
    high = decay.astype(BF16)
    low = (decay - high.astype(F32)).astype(BF16)
    carry = jnp.zeros((1, width), F32)
    pieces = []
    for start in range(0, rows, CHUNK):
        both = dot(
            lower,
            jnp.concatenate([high[start : start + CHUNK], low[start : start + CHUNK]], axis=1),
        )
        piece = both[:, :width] + both[:, width:] + carry
        carry = piece[CHUNK - 1 : CHUNK]
        pieces.append(piece)
    return jnp.concatenate(pieces, axis=0)


TAIL = 16


def recurrence_kernel(
    heads,
    q_ref,
    ff_ref,
    fb_ref,
    v_ref,
    lf_ref,
    lb_ref,
    extra_ref,
    out_ref,
    reach_f_ref,
    reach_b_ref,
    total_ref,
    mix_ref,
):
    rows = q_ref.shape[0]
    width = q_ref.shape[1] // heads
    row = lax.broadcasted_iota(jnp.int32, (CHUNK, CHUNK), 0)
    col = lax.broadcasted_iota(jnp.int32, (CHUNK, CHUNK), 1)
    lower = jnp.where(row >= col, 1.0, 0.0).astype(BF16)
    decays = [[], []]
    for head in range(heads):
        lanes = slice(head * width, (head + 1) * width)
        q = q_ref[:, lanes].astype(F32)
        q = q / (1.0 + jnp.exp(-q))
        v = v_ref[:, lanes]
        extra = jnp.transpose(jnp.broadcast_to(extra_ref[head : head + 1, :], (width, rows)))
        kf, gf = gate_terms(ff_ref[:, lanes], lf_ref[:, lanes], extra)
        kb, gb = gate_terms(fb_ref[:, lanes], lb_ref[:, lanes], extra)
        b = running_sum(gf, lower)
        total_f = b[rows - 1 : rows]
        ahead = running_sum(gb, lower)
        total_b = ahead[rows - 1 : rows]
        c = total_b - ahead + gb

        half = rows // 2
        while half >= CHUNK:
            for first in range(0, rows, 2 * half):
                mid, last = first + half, first + 2 * half
                one, two = slice(first, mid), slice(mid, last)
                ref_f, ref_b = b[mid - 1 : mid], c[mid : mid + 1]
                mix_ref[two, one] = dot(
                    (q[two] * jnp.exp(b[two] - ref_f)).astype(BF16),
                    (kf[one] * jnp.exp(ref_f - b[one])).astype(BF16),
                    NT,
                ).astype(BF16)
                mix_ref[one, two] = dot(
                    (q[one] * jnp.exp(c[one] - ref_b)).astype(BF16),
                    (kb[two] * jnp.exp(ref_b - c[two])).astype(BF16),
                    NT,
                ).astype(BF16)
            half //= 2
        for start in range(0, rows, CHUNK):
            here = slice(start, start + CHUNK)
            qc, kfc, kbc, bc, cc = q[here], kf[here], kb[here], b[here], c[here]
            mid_f, mid_b = [], []
            for first in range(0, CHUNK, FINE):
                at = first + FINE // 2
                mid_f.append(jnp.broadcast_to(bc[at - 1 : at], (FINE, width)))
                mid_b.append(jnp.broadcast_to(cc[at : at + 1], (FINE, width)))
            df = bc - jnp.concatenate(mid_f, axis=0)
            db = cc - jnp.concatenate(mid_b, axis=0)
            near_f = dot((qc * jnp.exp(df)).astype(BF16), (kfc * jnp.exp(-df)).astype(BF16), NT)
            near_b = dot((qc * jnp.exp(db)).astype(BF16), (kbc * jnp.exp(-db)).astype(BF16), NT)
            scores = jnp.where(row >= col, near_f, 0.0) + jnp.where(row <= col, near_b, 0.0)
            half = FINE
            while half < CHUNK:
                q_side, k_side = [], []
                for first in range(0, CHUNK, 2 * half):
                    mid, last = first + half, first + 2 * half
                    one, two = slice(first, mid), slice(mid, last)
                    ref_f, ref_b = bc[mid - 1 : mid], cc[mid : mid + 1]
                    q_side.append(qc[one] * jnp.exp(cc[one] - ref_b))
                    q_side.append(qc[two] * jnp.exp(bc[two] - ref_f))
                    k_side.append(kfc[one] * jnp.exp(ref_f - bc[one]))
                    k_side.append(kbc[two] * jnp.exp(ref_b - cc[two]))
                far = dot(
                    jnp.concatenate(q_side, axis=0).astype(BF16),
                    jnp.concatenate(k_side, axis=0).astype(BF16),
                    NT,
                )
                scores = jnp.where(row // half == col // half, scores, far)
                half *= 2
            mix_ref[here, here] = scores.astype(BF16)
        out_ref[:, lanes] = dot(mix_ref[...], v)
        reach_f_ref[:, lanes] = (q * jnp.exp(b)).astype(BF16)
        reach_b_ref[:, lanes] = (q * jnp.exp(c)).astype(BF16)
        for which, key, run, total in ((0, kf, b, total_f), (1, kb, c, total_b)):
            state = dot(v, (key * jnp.exp(total - run)).astype(BF16), TN)
            total_ref[which, lanes, :] = state.astype(BF16)
            decays[which].append(total)
    for which in range(2):
        put_decays(total_ref.at[which], decays[which])


def put_decays(message_ref, decays):
    heads = len(decays)
    edge, width = message_ref.shape[0] - TAIL, message_ref.shape[1]
    row = lax.broadcasted_iota(jnp.int32, (TAIL, width), 0)
    block = jnp.zeros((TAIL, width), F32)
    for head, decay in enumerate(decays):
        high = decay.astype(BF16).astype(F32)
        block = jnp.where(row == head, high, block)
        block = jnp.where(row == heads + head, decay - high, block)
    message_ref[edge:, :] = block.astype(BF16)


def get_decays(message, heads):
    block = message[message.shape[0] - TAIL :, :].astype(F32)
    return [block[head : head + 1] + block[heads + head : heads + head + 1] for head in range(heads)]


def join_kernel(bit, heads, first, single, me_ref, own_ref, other_ref, *refs):
    if first:
        send_ref, before_ref = refs
    else:
        old_ref, send_ref, before_ref = refs
    width = own_ref.shape[2]
    edge = heads * width
    upper = (me_ref[0] & bit) != 0
    send_back = (me_ref[0] & (2 * bit)) != 0
    zero = jnp.zeros((1, width), F32)
    for which in range(2):
        own, other = own_ref[which], other_ref[which]
        own_decay, other_decay = get_decays(own, heads), get_decays(other, heads)
        leads = upper if which == 0 else jnp.logical_not(upper)
        out = send_ref if single else send_ref.at[which]
        write = send_back if which == 1 else jnp.logical_not(send_back)
        tail_row = lax.broadcasted_iota(jnp.int32, (TAIL, width), 0)
        tail = jnp.zeros((TAIL, width), F32)
        both = []
        for head in range(heads):
            lanes = slice(head * width, (head + 1) * width)
            mine, theirs = own[lanes].astype(F32), other[lanes].astype(F32)
            late = jnp.where(leads, own_decay[head], other_decay[head])
            early_state = jnp.where(leads, theirs, mine)
            late_state = jnp.where(leads, mine, theirs)
            both.append((jnp.exp(late) * early_state + late_state).astype(BF16))
            held_decay = zero if first else old_ref[which, edge + head : edge + head + 1, :]
            held = jnp.zeros_like(mine) if first else old_ref[which, lanes, :]
            passed = jnp.exp(held_decay) * theirs + held
            before_ref[which, lanes, :] = jnp.where(leads, passed, held)
            reach = jnp.where(leads, held_decay + other_decay[head], held_decay)
            tail = jnp.where(tail_row == head, reach, tail)
        before_ref[which, edge:, :] = tail
        sums = [mine + theirs for mine, theirs in zip(own_decay, other_decay)]

        def put(out=out, both=both, sums=sums):
            for head in range(heads):
                out[head * width : (head + 1) * width, :] = both[head]
            put_decays(out, sums)

        if single:
            pl.when(write)(put)
        else:
            put()


def finish_kernel(
    bit,
    tp,
    heads,
    me_ref,
    quarter_ref,
    out_ref,
    reach_f_ref,
    reach_b_ref,
    gate_ref,
    gain_ref,
    w_ref,
    other_ref,
    before_ref,
    *refs,
):
    pieces = refs[:tp]
    hidden_ref = refs[tp]
    rows = out_ref.shape[0]
    width = out_ref.shape[1] // heads
    edge = heads * width
    quarter = quarter_ref[0]
    upper = (me_ref[0] & bit) != 0
    for head in range(heads):
        lanes = slice(head * width, (head + 1) * width)
        other = other_ref[lanes, :].astype(F32)
        combined = out_ref[:, lanes]
        for which, reach_ref in ((0, reach_f_ref), (1, reach_b_ref)):
            leads = upper if which == 0 else jnp.logical_not(upper)
            held = before_ref[which, lanes, :]
            passed = jnp.exp(before_ref[which, edge + head : edge + head + 1, :]) * other + held
            incoming = jnp.where(leads, passed, held).astype(BF16)
            combined += dot(reach_ref[:, lanes], incoming, NT)
        square = jnp.mean(combined * combined, axis=-1, keepdims=True)
        gate = gate_ref[:, lanes].astype(F32)
        gate = gate / (1.0 + jnp.exp(-gate))
        scaled = combined * lax.rsqrt(square + EPS) * gain_ref[:, lanes]
        hidden_ref[:, lanes] = (scaled * gate).astype(BF16)
    block = rows // tp
    for piece in range(tp):
        start = pl.multiple_of((quarter ^ piece) * block, block)
        part = hidden_ref[pl.ds(start, block), :]
        pieces[piece][...] = dot(part, w_ref[...]).astype(BF16)


def swap(array, axis, bit):
    size = lax.axis_size(axis)
    return lax.ppermute(array, axis, [(place, place ^ bit) for place in range(size)])


def gather_quarters(own, axis):
    size = lax.axis_size(axis)
    pieces = {0: own}
    bit = size // 2
    while bit:
        for held in list(pieces):
            pieces[held | bit] = swap(pieces[held], axis, bit)
        bit //= 2
    return [pieces[place] for place in range(size)]


def scatter_sum(pieces, axis):
    size = lax.axis_size(axis)
    sums = {place: piece for place, piece in enumerate(pieces)}
    bit = 1
    while bit < size:
        going = [place for place in sums if place & bit]
        arrived = [swap(sums[place].astype(BF16), axis, bit) for place in going]
        for place, piece in zip(going, arrived):
            del sums[place]
            sums[place ^ bit] = sums[place ^ bit].astype(F32) + piece.astype(F32)
        bit *= 2
    return sums[0].astype(BF16)


def routing_kernel(groups, experts, me_ref, quarter_ref, rows_ref, gain_ref, routes_ref, *outs):
    count, _ = rows_ref.shape
    slots = 2 * TOPK * count // experts
    per_group = experts * slots // groups
    wide = rows_ref[...].astype(F32)
    square = jnp.mean(wide * wide, axis=-1, keepdims=True)
    normed = (wide * lax.rsqrt(square + EPS) * gain_ref[...]).astype(BF16)
    row = lax.broadcasted_iota(jnp.int32, (count, count), 0)
    col = lax.broadcasted_iota(jnp.int32, (count, count), 1)
    before = jnp.where(row < col, 1.0, 0.0).astype(BF16)
    expert = lax.broadcasted_iota(jnp.int32, (experts, count), 0)
    member = routes_ref[0:1, :] == expert
    for k in range(1, TOPK):
        member = jnp.logical_or(member, routes_ref[k : k + 1, :] == expert)
    rank = dot(jnp.where(member, 1.0, 0.0).astype(BF16), before)
    rank = jnp.where(member, rank, -1.0).astype(BF16)
    for group, out_ref in enumerate(outs):
        slot = group * per_group + lax.broadcasted_iota(jnp.int32, (per_group, experts), 0)
        which = lax.broadcasted_iota(jnp.int32, (per_group, experts), 1)
        owner = slot // slots
        if groups > 1:
            owner = owner ^ me_ref[0]
        ranks = dot(jnp.where(owner == which, 1.0, 0.0).astype(BF16), rank)
        place = lax.broadcasted_iota(jnp.int32, (per_group, count), 0) % slots
        pick = jnp.where(ranks == place.astype(F32), 1.0, 0.0).astype(BF16)
        out_ref[...] = dot(pick, normed).astype(BF16)


def picks_kernel(groups, experts, me_ref, quarter_ref, routes_ref, factor_ref, pick_ref, weight_ref):
    count = routes_ref.shape[1]
    slots = 2 * TOPK * count // experts
    row = lax.broadcasted_iota(jnp.int32, (count, count), 0)
    col = lax.broadcasted_iota(jnp.int32, (count, count), 1)
    before = jnp.where(row > col, 1.0, 0.0).astype(BF16)

    def column(line):
        return jnp.transpose(jnp.broadcast_to(line, (count, count)))

    named = [column(routes_ref[k : k + 1, :]) for k in range(TOPK)]
    hits = [named[k] == col for k in range(TOPK)]
    member = hits[0]
    for k in range(1, TOPK):
        member = jnp.logical_or(member, hits[k])
    rank = dot(before, jnp.where(member, 1.0, 0.0).astype(BF16))
    slot = lax.broadcasted_iota(jnp.int32, (count, experts * slots), 1)
    for k in range(TOPK):
        place = jnp.sum(jnp.where(hits[k], rank, 0.0), axis=1, keepdims=True).astype(jnp.int32)
        owner = named[k][:, :1]
        if groups > 1:
            owner = owner ^ me_ref[0]
        rows = slice(k * count, (k + 1) * count)
        pick_ref[rows, :] = jnp.where(slot == owner * slots + place, 1.0, 0.0).astype(BF16)
        weight_ref[rows, :] = column(factor_ref[k : k + 1, :])


def hidden_kernel(groups, parts, *refs):
    xs = refs[:groups]
    gates = refs[groups : groups + parts]
    ups = refs[groups + parts : groups + 2 * parts]
    out_ref = refs[-1]
    width = gates[0].shape[1]
    x = jnp.concatenate([one[...] for one in xs], axis=0)
    for i in range(parts):
        gated = dot(x, gates[i][...])
        lifted = dot(x, ups[i][...])
        opened = gated / (1.0 + jnp.exp(-gated))
        out_ref[:, i * width : (i + 1) * width] = (opened * lifted).astype(BF16)


def down_kernel(groups, parts, hidden_ref, *refs):
    downs, outs = refs[:parts], refs[parts:]
    depth, width = downs[0].shape
    rows = hidden_ref.shape[0] // groups
    for first in range(0, width, TILE):
        lanes = slice(first, min(first + TILE, width))
        total = None
        for i in range(parts):
            term = dot(hidden_ref[:, i * depth : (i + 1) * depth], downs[i][:, lanes])
            total = term if total is None else total + term
        result = total.astype(BF16)
        for group, out_ref in enumerate(outs):
            out_ref[:, lanes] = result[group * rows : (group + 1) * rows]


def blend_kernel(groups, pick_ref, weight_ref, *refs):
    arrived = refs[:groups]
    out_ref = refs[-1]
    count = out_ref.shape[0]
    results = jnp.concatenate([one[...] for one in arrived], axis=0)
    chosen = dot(pick_ref[...], results)
    total = None
    for k in range(TOPK):
        rows = slice(k * count, (k + 1) * count)
        term = chosen[rows] * weight_ref[rows, :1]
        total = term if total is None else total + term
    done = 0
    for earlier in refs[groups:-1]:
        out_ref[:, done : done + earlier.shape[1]] = earlier[...]
        done += earlier.shape[1]
    out_ref[:, done : done + total.shape[1]] = total.astype(BF16)


def call(kernel, operands, room=12, **options):
    return pl.pallas_call(kernel, compiler_params=params(room), **options)(*operands)


def shards(
    queries,
    forget_forward_logits,
    forget_backward_logits,
    values,
    output_gate_logits,
    lower_bound_forward,
    lower_bound_backward,
    extra_log_decay,
    head_norm_scale,
    output_projection,
    second_residual,
    expert_norm_scale,
    routes,
    specialist_mixing_factor,
    expert_gate_matrix,
    expert_up_matrix,
    expert_down_matrix,
):
    ep, tp = lax.axis_size("ep"), lax.axis_size("tp")
    direct = ep <= DIRECT_EP
    groups = ep if direct else 1
    me = lax.axis_index("ep").reshape(1).astype(jnp.int32)
    quarter = lax.axis_index("tp").reshape(1).astype(jnp.int32)
    rows_all, model = second_residual.shape
    count = rows_all // tp
    capacity = 2 * TOPK * count
    per_group = capacity // groups
    depth = expert_gate_matrix.shape[2]
    shape = jax.ShapeDtypeStruct
    routes_t = routes.T
    factor_t = specialist_mixing_factor.T

    gates = gather_quarters(expert_gate_matrix[0], "tp")
    ups = gather_quarters(expert_up_matrix[0], "tp")
    edges = [0]
    for share in DOWN_EIGHTHS:
        edges.append(edges[-1] + model * share // sum(DOWN_EIGHTHS))
    parts = list(zip(edges, edges[1:]))
    downs = [gather_quarters(expert_down_matrix[0, :, start:stop], "tp") for start, stop in parts]

    def whole(grid_index, a, b):
        return (0, 0)

    outgoing = call(
        functools.partial(routing_kernel, groups, ep),
        (me, quarter, second_residual, expert_norm_scale.reshape(1, -1), routes_t),
        grid_spec=pltpu.PrefetchScalarGridSpec(
            num_scalar_prefetch=2,
            grid=(1,),
            in_specs=[
                pl.BlockSpec((count, model), lambda i, a, b: (b[0], 0)),
                pl.BlockSpec((1, model), whole),
                pl.BlockSpec((TOPK, count), lambda i, a, b: (0, b[0])),
            ],
            out_specs=[pl.BlockSpec((per_group, model), whole)] * groups,
        ),
        out_shape=[shape((per_group, model), BF16)] * groups,
        cost_estimate=cost(2 * capacity * count * model, 2 * (count + capacity) * model),
    )

    def exchange(blocks):
        if direct:
            return {
                step: swap(block, "ep", step) if step else block
                for step, block in blocks.items()
            }
        stacked = blocks[0].reshape(ep, capacity // ep, -1)
        moved = lax.all_to_all(stacked, "ep", split_axis=0, concat_axis=0, tiled=True)
        return {0: moved.reshape(capacity, -1)}

    arrived = exchange(dict(enumerate(outgoing)))

    rows, key_width = queries.shape
    heads = extra_log_decay.shape[1]
    message = (key_width + TAIL, key_width // heads)
    inner, reach_f, reach_b, total = call(
        functools.partial(recurrence_kernel, heads),
        (
            queries,
            forget_forward_logits,
            forget_backward_logits,
            values,
            lower_bound_forward.reshape(1, -1),
            lower_bound_backward.reshape(1, -1),
            extra_log_decay.T,
        ),
        in_specs=[VM] * 7,
        out_specs=[VM] * 4,
        out_shape=[
            shape((rows, key_width), F32),
            shape((rows, key_width), BF16),
            shape((rows, key_width), BF16),
            shape((2,) + message, BF16),
        ],
        scratch_shapes=[pltpu.VMEM((rows, rows), BF16)],
        cost_estimate=cost(12e9, 8 * rows * key_width, 20 * rows * key_width),
    )
    bit = 1
    before = None
    while bit < ep:
        other = swap(total, "ep", bit)
        if 2 * bit < ep:
            single = 4 * bit >= ep
            total, before = call(
                functools.partial(join_kernel, bit, heads, before is None, single),
                (me, total, other) + (() if before is None else (before,)),
                in_specs=[SM] + [VM] * (2 if before is None else 3),
                out_specs=[VM] * 2,
                out_shape=[
                    shape(message if single else (2,) + message, BF16),
                    shape((2,) + message, F32),
                ],
                cost_estimate=cost(4 * key_width * key_width, 8 * key_width * key_width),
            )
        bit *= 2

    hidden = call(
        functools.partial(hidden_kernel, groups, tp),
        [arrived[step] for step in range(groups)] + gates + ups,
        room=24,
        in_specs=[VM] * (groups + 2 * tp),
        out_specs=VM,
        out_shape=shape((capacity, tp * depth), BF16),
        cost_estimate=cost(4 * capacity * model * tp * depth, 4 * model * tp * depth),
    )
    returned = []
    for i, (start, stop) in enumerate(parts):
        wide = stop - start
        results = call(
            functools.partial(down_kernel, groups, tp),
            [hidden] + downs[i],
            in_specs=[VM] * (1 + tp),
            out_specs=[VM] * groups,
            out_shape=[shape((per_group, wide), BF16)] * groups,
            cost_estimate=cost(2 * capacity * tp * depth * wide, 2 * tp * depth * wide),
        )
        returned.append(exchange(dict(enumerate(results))))

    mixed = call(
        functools.partial(finish_kernel, ep // 2, tp, heads),
        (
            me,
            quarter,
            inner,
            reach_f,
            reach_b,
            output_gate_logits,
            head_norm_scale.reshape(1, -1),
            output_projection,
            other,
            before,
        ),
        in_specs=[SM, SM] + [VM] * 8,
        out_specs=[VM] * tp,
        out_shape=[shape((rows // tp, model), BF16)] * tp,
        scratch_shapes=[pltpu.VMEM((rows, key_width), BF16)],
        cost_estimate=cost(2 * rows * key_width * model, 6 * rows * model, rows * key_width),
    )
    mixer_output = scatter_sum(mixed, "tp")

    pick, weight = call(
        functools.partial(picks_kernel, groups, ep),
        (me, quarter, routes_t, factor_t),
        grid_spec=pltpu.PrefetchScalarGridSpec(
            num_scalar_prefetch=2,
            grid=(1,),
            in_specs=[
                pl.BlockSpec((TOPK, count), lambda i, a, b: (0, b[0])),
                pl.BlockSpec((TOPK, count), whole),
            ],
            out_specs=[
                pl.BlockSpec((TOPK * count, capacity), whole),
                pl.BlockSpec((TOPK * count, count), whole),
            ],
        ),
        out_shape=[shape((TOPK * count, capacity), BF16), shape((TOPK * count, count), F32)],
        cost_estimate=cost(4 * count * count * count, 2 * TOPK * count * capacity),
    )
    ready = []
    for i, (start, stop) in enumerate(parts):
        last = i == len(parts) - 1
        if last:
            pick, mixer_output = lax.optimization_barrier((pick, mixer_output))
        blocks = [returned[i][step] for step in range(groups)]
        ready.append(
            call(
                functools.partial(blend_kernel, groups),
                (pick, weight, *blocks, *(ready if last else [])),
                in_specs=[VM] * (2 + groups + (i if last else 0)),
                out_specs=VM,
                out_shape=shape((count, model if last else stop - start), BF16),
                cost_estimate=cost(
                    2 * TOPK * count * capacity * (stop - start), 2 * capacity * (stop - start)
                ),
            )
        )
    return (mixer_output, ready[-1])


def solution(mesh):
    in_specs = (
        P("ep", "tp"),
        P("ep", "tp"),
        P("ep", "tp"),
        P("ep", "tp"),
        P("ep", "tp"),
        P("tp"),
        P("tp"),
        P("ep", "tp"),
        P("tp"),
        P("tp", None),
        P("ep", None),
        P(),
        P("ep", None),
        P(("ep", "tp"), None),
        P("ep", None, "tp"),
        P("ep", None, "tp"),
        P("ep", "tp", None),
    )
    out_specs = (P(("ep", "tp"), None), P(("ep", "tp"), None))
    return jax.shard_map(shards, mesh=mesh, in_specs=in_specs, out_specs=out_specs, check_vma=False)
```

time: 193 us -> 201 us (1.041)
  Pallas kernels: 44.2 us -> 15.7 us
  waiting for transfers between devices: 74.8 us -> 99.5 us
  starting transfers between devices: 62.8 us -> 73.8 us
    pallas_call x10 -> x11, Pallas kernels: 44.2 us -> 15.7 us  [call(): pl.pallas_call(kernel, compiler_params=params(room), **options)(*operands)]
    ppermute x40 -> x39, waiting for transfers between devices: 74.8 us -> 99.5 us  [swap(): lax.ppermute(array, axis, [(place, place ^ bit) for place in range(size)])]
    ppermute x40 -> x39, starting transfers between devices: 62.8 us -> 73.8 us  [swap(): lax.ppermute(array, axis, [(place, place ^ bit) for place in range(size)])]
    squeeze x1 -> x2, local copies, waits for them, and re-layouts: 0.08 us -> 2.15 us  [shards(): expert_down_matrix[0, :, start:stop]]
    unnamed x88 -> x32, local copies, waits for them, and re-layouts: 6.64 us -> 5.88 us
  transfers between devices with their start and end apart: 40 -> 39, of which waited for: 13 -> 9; matrix products, arithmetic and copies ran while one was open for 1% -> 2% of each run, Pallas kernels for 19% -> 6%
where the time goes in v1:
time: 201 us; the launch traced here: 199 us
  waiting for transfers between devices  99.5 us (50%)
  starting transfers between devices  73.8 us (37%)
  Pallas kernels  15.7 us (8%)
  local copies, waits for them, and re-layouts  8.03 us (4%)
    ppermute x39, waiting for transfers between devices, swap(): lax.ppermute(array, axis, [(place, place ^ bit) for place in range(size)])  99.5 us
    ppermute x39, starting transfers between devices, swap(): lax.ppermute(array, axis, [(place, place ^ bit) for place in range(size)])  73.8 us
    pallas_call x11, Pallas kernels, call(): pl.pallas_call(kernel, compiler_params=params(room), **options)(*operands)  15.7 us
    unnamed x32, local copies, waits for them, and re-layouts  5.88 us
  transfers between devices with their start and end apart: 39, of which 9 were waited for; matrix products, arithmetic and copies ran while one was open for 2% of the time, Pallas kernels for 6%

profile of v1, /device:TPU:0, one launch (start us, length us, event | category | flops | bytes accessed | tf_op | source)
XLA Modules:
  0.0 199.1 jit_solution(13614437298630958691)
XLA Ops:
  6.5 3.0 %shard_map.177 = (f32[512,256]{1,0:T(8,128)S(1)}, bf16[512,256]{1,0:T(8,128)(2,1)S(1)}, bf16[512,256]{1,0:T(8,128)(2,1)S(1)}, bf16[2,272,128]{2,1,0:T(8,128)(2,1)S(1)}) custom-call(bf16[512,256]{1,0:T(8,128)(2,1)S(1)} %copy-done.8, bf16[512,256]{1,0:T(8,128)(2,1)S(1)} %copy-done.9, bf16[512,256]{1,0:T(8,128)(2,1)S(1)} %copy-done.10, ...), custom_call_target="tpu_custom_call" | custom-call | flops 12000000000 | bytes 1048576 | tf_op jit(solution)/shard_map/pallas_call | solution.py:403
  9.5 3.0 %collective-permute-start = (bf16[2,272,128]{2,1,0:T(8,128)(2,1)S(1)}, bf16[2,272,128]{2,1,0:T(8,128)(2,1)S(1)}, u32[]{:S(2)}, u32[]{:S(2)}) collective-permute-start(bf16[2,272,128]{2,1,0:T(8,128)(2,1)S(1)} %get-tuple-element.46.own_ref), channel_id=1, source_target_pairs={{0,4},{4,0},{8,12},{12,8},{16,20},{20,16},{24,28},{28,24},{1,5},{5... | collective-permute-start | bytes 417800 | tf_op jit(solution)/shard_map/ppermute | solution.py:272
  12.6 1.9 shard_map.181
  14.5 2.6 %collective-permute-start.10 = (bf16[64,2048]{1,0:T(8,128)(2,1)S(1)}, bf16[64,2048]{1,0:T(8,128)(2,1)S(1)}, u32[]{:S(2)}, u32[]{:S(2)}) collective-permute-start(bf16[64,2048]{1,0:T(8,128)(2,1)S(1)} %get-tuple-element.63), channel_id=1, source_target_pairs={{0,20},{4,16},{8,28},{12,24},{16,4},{20,0},{24,12},{28,8},{1,21},{... | collective-permute-start | bytes 786440 | tf_op jit(solution)/shard_map/ppermute | solution.py:272
  17.2 1.3 collective-permute-start.11
  18.5 3.4 %collective-permute-start.12 = (bf16[64,2048]{1,0:T(8,128)(2,1)S(1)}, bf16[64,2048]{1,0:T(8,128)(2,1)S(1)}, u32[]{:S(2)}, u32[]{:S(2)}) collective-permute-start(bf16[64,2048]{1,0:T(8,128)(2,1)S(1)} %get-tuple-element.65), channel_id=1, source_target_pairs={{0,28},{4,24},{8,20},{12,16},{16,12},{20,8},{24,4},{28,0},{1,29},{... | collective-permute-start | bytes 786440 | tf_op jit(solution)/shard_map/ppermute | solution.py:272
  22.5 19.6 %collective-permute-done.10.refs_5_ = bf16[64,2048]{1,0:T(8,128)(2,1)S(1)} collective-permute-done((bf16[64,2048]{1,0:T(8,128)(2,1)S(1)}, bf16[64,2048]{1,0:T(8,128)(2,1)S(1)}, u32[]{:S(2)}, u32[]{:S(2)}) %collective-permute-start.10) | collective-permute-done | bytes 262176 | tf_op jit(solution)/shard_map/ppermute | solution.py:272
  42.2 6.3 %collective-permute-start.9 = (bf16[64,2048]{1,0:T(8,128)(2,1)S(1)}, bf16[64,2048]{1,0:T(8,128)(2,1)S(1)}, u32[]{:S(2)}, u32[]{:S(2)}) collective-permute-start(bf16[64,2048]{1,0:T(8,128)(2,1)S(1)} %get-tuple-element.62), channel_id=1, source_target_pairs={{0,16},{4,20},{8,24},{12,28},{16,0},{20,4},{24,8},{28,12},{1,17},{... | collective-permute-start | bytes 786440 | tf_op jit(solution)/shard_map/ppermute | solution.py:272
  48.5 1.5 collective-permute-start.14
  50.5 12.5 %collective-permute-start.1 = (bf16[2,272,128]{2,1,0:T(8,128)(2,1)S(1)}, bf16[2,272,128]{2,1,0:T(8,128)(2,1)S(1)}, u32[]{:S(2)}, u32[]{:S(2)}) collective-permute-start(bf16[2,272,128]{2,1,0:T(8,128)(2,1)S(1)} %get-tuple-element.47.own_ref), channel_id=1, source_target_pairs={{0,8},{4,12},{8,0},{12,4},{16,24},{20,28},{24,16},{28,20},{1,9},{5... | collective-permute-start | bytes 417800 | tf_op jit(solution)/shard_map/ppermute | solution.py:272
  64.1 3.8 %collective-permute-done.1.other_ref = bf16[2,272,128]{2,1,0:T(8,128)(2,1)S(1)} collective-permute-done((bf16[2,272,128]{2,1,0:T(8,128)(2,1)S(1)}, bf16[2,272,128]{2,1,0:T(8,128)(2,1)S(1)}, u32[]{:S(2)}, u32[]{:S(2)}) %collective-permute-start.1) | collective-permute-done | bytes 139296 | tf_op jit(solution)/shard_map/ppermute | solution.py:272
  67.9 1.5 collective-permute-start.30
  72.0 4.7 %collective-permute-done.2.other_ref = bf16[272,128]{1,0:T(8,128)(2,1)S(1)} collective-permute-done((bf16[272,128]{1,0:T(8,128)(2,1)S(1)}, bf16[272,128]{1,0:T(8,128)(2,1)S(1)}, u32[]{:S(2)}, u32[]{:S(2)}) %collective-permute-start.2) | collective-permute-done | bytes 69664 | tf_op jit(solution)/shard_map/ppermute | solution.py:272
  77.2 40.9 %collective-permute-done.20.refs_2_ = bf16[256,768]{1,0:T(8,128)(2,1)S(1)} collective-permute-done((bf16[256,768]{1,0:T(8,128)(2,1)S(1)}, bf16[256,768]{1,0:T(8,128)(2,1)S(1)}, u32[]{:S(2)}, u32[]{:S(2)}) %collective-permute-start.20) | collective-permute-done | bytes 393248 | tf_op jit(solution)/shard_map/ppermute | solution.py:272
  119.1 1.2 shard_map.180
  120.5 5.5 %collective-permute-done.4 = bf16[128,2048]{1,0:T(8,128)(2,1)S(1)} collective-permute-done((bf16[128,2048]{1,0:T(8,128)(2,1)S(1)}, bf16[128,2048]{1,0:T(8,128)(2,1)S(1)}, u32[]{:S(2)}, u32[]{:S(2)}) %collective-permute-start.4) | collective-permute-done | bytes 524320 | tf_op jit(solution)/shard_map/ppermute | solution.py:272
  127.3 1.5 collective-permute-start.5
  128.8 4.5 %shard_map.182.hidden_ref = bf16[512,1024]{1,0:T(8,128)(2,1)S(1)} custom-call(bf16[64,2048]{1,0:T(8,128)(2,1)S(1)} %get-tuple-element.58.refs_0_, bf16[64,2048]{1,0:T(8,128)(2,1)S(1)} %collective-permute-done.6.refs_1_, bf16[64,2048]{1,0:T(8,128)(2,1)S(1)} %collective-permute-done.7.refs_2_, bf16[64,2048]{1,0:T(8,128)(2,1)S(1)} %collective-permute-done.8.refs_3_, ...), custom_call_target="tpu_custom_call" | custom-call | flops 4294967296 | bytes 8388608 | tf_op jit(solution)/shard_map/pallas_call | solution.py:403
  133.3 1.5 shard_map.184
  134.9 1.5 collective-permute-start.32
  136.4 10.9 %collective-permute-start.33 = (bf16[64,1280]{1,0:T(8,128)(2,1)S(1)}, bf16[64,1280]{1,0:T(8,128)(2,1)S(1)}, u32[]{:S(2)}, u32[]{:S(2)}) collective-permute-start(bf16[64,1280]{1,0:T(8,128)(2,1)S(1)} %get-tuple-element.76), channel_id=1, source_target_pairs={{0,8},{4,12},{8,0},{12,4},{16,24},{20,28},{24,16},{28,20},{1,9},{5... | collective-permute-start | bytes 491528 | tf_op jit(solution)/shard_map/ppermute | solution.py:272
  149.0 4.0 %collective-permute-start.34 = (bf16[64,1280]{1,0:T(8,128)(2,1)S(1)}, bf16[64,1280]{1,0:T(8,128)(2,1)S(1)}, u32[]{:S(2)}, u32[]{:S(2)}) collective-permute-start(bf16[64,1280]{1,0:T(8,128)(2,1)S(1)} %get-tuple-element.77), channel_id=1, source_target_pairs={{0,12},{4,8},{8,4},{12,0},{16,28},{20,24},{24,20},{28,16},{1,13},{... | collective-permute-start | bytes 491528 | tf_op jit(solution)/shard_map/ppermute | solution.py:272
  153.0 3.7 %collective-permute-start.35 = (bf16[64,1280]{1,0:T(8,128)(2,1)S(1)}, bf16[64,1280]{1,0:T(8,128)(2,1)S(1)}, u32[]{:S(2)}, u32[]{:S(2)}) collective-permute-start(bf16[64,1280]{1,0:T(8,128)(2,1)S(1)} %get-tuple-element.78), channel_id=1, source_target_pairs={{0,16},{4,20},{8,24},{12,28},{16,0},{20,4},{24,8},{28,12},{1,17},{... | collective-permute-start | bytes 491528 | tf_op jit(solution)/shard_map/ppermute | solution.py:272
  156.7 1.4 collective-permute-start.36
  158.1 2.1 %collective-permute-start.37 = (bf16[64,1280]{1,0:T(8,128)(2,1)S(1)}, bf16[64,1280]{1,0:T(8,128)(2,1)S(1)}, u32[]{:S(2)}, u32[]{:S(2)}) collective-permute-start(bf16[64,1280]{1,0:T(8,128)(2,1)S(1)} %get-tuple-element.80), channel_id=1, source_target_pairs={{0,24},{4,28},{8,16},{12,20},{16,8},{20,12},{24,0},{28,4},{1,25},{... | collective-permute-start | bytes 491528 | tf_op jit(solution)/shard_map/ppermute | solution.py:272
  160.2 1.7 collective-permute-start.38
  162.9 13.3 %collective-permute-done.35.refs_4_ = bf16[64,1280]{1,0:T(8,128)(2,1)S(1)} collective-permute-done((bf16[64,1280]{1,0:T(8,128)(2,1)S(1)}, bf16[64,1280]{1,0:T(8,128)(2,1)S(1)}, u32[]{:S(2)}, u32[]{:S(2)}) %collective-permute-start.35) | collective-permute-done | bytes 163872 | tf_op jit(solution)/shard_map/ppermute | solution.py:272
  176.2 2.0 %collective-permute-done.36.refs_5_ = bf16[64,1280]{1,0:T(8,128)(2,1)S(1)} collective-permute-done((bf16[64,1280]{1,0:T(8,128)(2,1)S(1)}, bf16[64,1280]{1,0:T(8,128)(2,1)S(1)}, u32[]{:S(2)}, u32[]{:S(2)}) %collective-permute-start.36) | collective-permute-done | bytes 163872 | tf_op jit(solution)/shard_map/ppermute | solution.py:272
  178.3 6.5 %collective-permute-start.27 = (bf16[64,768]{1,0:T(8,128)(2,1)S(1)}, bf16[64,768]{1,0:T(8,128)(2,1)S(1)}, u32[]{:S(2)}, u32[]{:S(2)}) collective-permute-start(bf16[64,768]{1,0:T(8,128)(2,1)S(1)} %get-tuple-element.72), channel_id=1, source_target_pairs={{0,24},{4,28},{8,16},{12,20},{16,8},{20,12},{24,0},{28,4},{1,25},{... | collective-permute-start | bytes 294920 | tf_op jit(solution)/shard_map/ppermute | solution.py:272
  184.8 2.0 %collective-permute-start.28 = (bf16[64,768]{1,0:T(8,128)(2,1)S(1)}, bf16[64,768]{1,0:T(8,128)(2,1)S(1)}, u32[]{:S(2)}, u32[]{:S(2)}) collective-permute-start(bf16[64,768]{1,0:T(8,128)(2,1)S(1)} %get-tuple-element.73), channel_id=1, source_target_pairs={{0,28},{4,24},{8,20},{12,16},{16,12},{20,8},{24,4},{28,0},{1,29},{... | collective-permute-start | bytes 294920 | tf_op jit(solution)/shard_map/ppermute | solution.py:272
  188.3 8.3 %collective-permute-done.25.refs_4_ = bf16[64,768]{1,0:T(8,128)(2,1)S(1)} collective-permute-done((bf16[64,768]{1,0:T(8,128)(2,1)S(1)}, bf16[64,768]{1,0:T(8,128)(2,1)S(1)}, u32[]{:S(2)}, u32[]{:S(2)}) %collective-permute-start.25) | collective-permute-done | bytes 98336 | tf_op jit(solution)/shard_map/ppermute | solution.py:272
  196.7 1.3 collective-permute-done.26.refs_5_
  (93 shorter events, 19.0 us)
Async XLA Ops:
  9.5 12.9 %collective-permute-start = (bf16[2,272,128]{2,1,0:T(8,128)(2,1)S(1)}, bf16[2,272,128]{2,1,0:T(8,128)(2,1)S(1)}, u32[]{:S(2)}, u32[]{:S(2)}) collective-permute-start(bf16[2,272,128]{2,1,0:T(8,128)(2,1)S(1)} %get-tuple-element.46.own_ref), channel_id=1, source_target_pairs={{0,4},{4,0},{8,12},{12,8},{16,20},{20,16},{24,28},{28,24},{1,5},{5... | collective-permute-start | bytes 417800 | tf_op jit(solution)/shard_map/ppermute | solution.py:272
  14.5 27.6 %collective-permute-start.10 = (bf16[64,2048]{1,0:T(8,128)(2,1)S(1)}, bf16[64,2048]{1,0:T(8,128)(2,1)S(1)}, u32[]{:S(2)}, u32[]{:S(2)}) collective-permute-start(bf16[64,2048]{1,0:T(8,128)(2,1)S(1)} %get-tuple-element.63), channel_id=1, source_target_pairs={{0,20},{4,16},{8,28},{12,24},{16,4},{20,0},{24,12},{28,8},{1,21},{... | collective-permute-start | bytes 786440 | tf_op jit(solution)/shard_map/ppermute | solution.py:272
  17.2 25.0 %collective-permute-start.11 = (bf16[64,2048]{1,0:T(8,128)(2,1)S(1)}, bf16[64,2048]{1,0:T(8,128)(2,1)S(1)}, u32[]{:S(2)}, u32[]{:S(2)}) collective-permute-start(bf16[64,2048]{1,0:T(8,128)(2,1)S(1)} %get-tuple-element.64), channel_id=1, source_target_pairs={{0,24},{4,28},{8,16},{12,20},{16,8},{20,12},{24,0},{28,4},{1,25},{... | collective-permute-start | bytes 786440 | tf_op jit(solution)/shard_map/ppermute | solution.py:272
  18.5 29.9 %collective-permute-start.12 = (bf16[64,2048]{1,0:T(8,128)(2,1)S(1)}, bf16[64,2048]{1,0:T(8,128)(2,1)S(1)}, u32[]{:S(2)}, u32[]{:S(2)}) collective-permute-start(bf16[64,2048]{1,0:T(8,128)(2,1)S(1)} %get-tuple-element.65), channel_id=1, source_target_pairs={{0,28},{4,24},{8,20},{12,16},{16,12},{20,8},{24,4},{28,0},{1,29},{... | collective-permute-start | bytes 786440 | tf_op jit(solution)/shard_map/ppermute | solution.py:272
  21.9 28.1 %collective-permute-start.6 = (bf16[64,2048]{1,0:T(8,128)(2,1)S(1)}, bf16[64,2048]{1,0:T(8,128)(2,1)S(1)}, u32[]{:S(2)}, u32[]{:S(2)}) collective-permute-start(bf16[64,2048]{1,0:T(8,128)(2,1)S(1)} %get-tuple-element.59), channel_id=1, source_target_pairs={{0,4},{4,0},{8,12},{12,8},{16,20},{20,16},{24,28},{28,24},{1,5},{5... | collective-permute-start | bytes 786440 | tf_op jit(solution)/shard_map/ppermute | solution.py:272
  22.5 28.0 %collective-permute-start.7 = (bf16[64,2048]{1,0:T(8,128)(2,1)S(1)}, bf16[64,2048]{1,0:T(8,128)(2,1)S(1)}, u32[]{:S(2)}, u32[]{:S(2)}) collective-permute-start(bf16[64,2048]{1,0:T(8,128)(2,1)S(1)} %get-tuple-element.60), channel_id=1, source_target_pairs={{0,8},{4,12},{8,0},{12,4},{16,24},{20,28},{24,16},{28,20},{1,9},{5... | collective-permute-start | bytes 786440 | tf_op jit(solution)/shard_map/ppermute | solution.py:272
  42.2 27.5 %collective-permute-start.8 = (bf16[64,2048]{1,0:T(8,128)(2,1)S(1)}, bf16[64,2048]{1,0:T(8,128)(2,1)S(1)}, u32[]{:S(2)}, u32[]{:S(2)}) collective-permute-start(bf16[64,2048]{1,0:T(8,128)(2,1)S(1)} %get-tuple-element.61), channel_id=1, source_target_pairs={{0,12},{4,8},{8,4},{12,0},{16,28},{20,24},{24,20},{28,16},{1,13},{... | collective-permute-start | bytes 786440 | tf_op jit(solution)/shard_map/ppermute | solution.py:272
  42.2 27.6 %collective-permute-start.9 = (bf16[64,2048]{1,0:T(8,128)(2,1)S(1)}, bf16[64,2048]{1,0:T(8,128)(2,1)S(1)}, u32[]{:S(2)}, u32[]{:S(2)}) collective-permute-start(bf16[64,2048]{1,0:T(8,128)(2,1)S(1)} %get-tuple-element.62), channel_id=1, source_target_pairs={{0,16},{4,20},{8,24},{12,28},{16,0},{20,4},{24,8},{28,12},{1,17},{... | collective-permute-start | bytes 786440 | tf_op jit(solution)/shard_map/ppermute | solution.py:272
  48.5 70.2 %collective-permute-start.14 = (bf16[2048,256]{1,0:T(8,128)(2,1)S(1)}, bf16[2048,256]{1,0:T(8,128)(2,1)S(1)}, u32[]{:S(2)}, u32[]{:S(2)}) collective-permute-start(bf16[2048,256]{1,0:T(8,128)(2,1)S(1)} %bitcast.19), channel_id=1, source_target_pairs={{0,2},{1,3},{2,0},{3,1},{4,6},{5,7},{6,4},{7,5},{8,10},{9,11},{10,... | collective-permute-start | bytes 3145736 | tf_op jit(solution)/shard_map/ppermute | solution.py:272
  50.0 68.7 %collective-permute-start.17 = (bf16[2048,256]{1,0:T(8,128)(2,1)S(1)}, bf16[2048,256]{1,0:T(8,128)(2,1)S(1)}, u32[]{:S(2)}, u32[]{:S(2)}) collective-permute-start(bf16[2048,256]{1,0:T(8,128)(2,1)S(1)} %bitcast.22), channel_id=1, source_target_pairs={{0,2},{1,3},{2,0},{3,1},{4,6},{5,7},{6,4},{7,5},{8,10},{9,11},{10,... | collective-permute-start | bytes 3145736 | tf_op jit(solution)/shard_map/ppermute | solution.py:272
  50.5 17.4 %collective-permute-start.1 = (bf16[2,272,128]{2,1,0:T(8,128)(2,1)S(1)}, bf16[2,272,128]{2,1,0:T(8,128)(2,1)S(1)}, u32[]{:S(2)}, u32[]{:S(2)}) collective-permute-start(bf16[2,272,128]{2,1,0:T(8,128)(2,1)S(1)} %get-tuple-element.47.own_ref), channel_id=1, source_target_pairs={{0,8},{4,12},{8,0},{12,4},{16,24},{20,28},{24,16},{28,20},{1,9},{5... | collective-permute-start | bytes 417800 | tf_op jit(solution)/shard_map/ppermute | solution.py:272
  67.9 50.2 %collective-permute-start.30 = (bf16[256,1280]{1,0:T(8,128)(2,1)S(1)}, bf16[256,1280]{1,0:T(8,128)(2,1)S(1)}, u32[]{:S(2)}, u32[]{:S(2)}) collective-permute-start(bf16[256,1280]{1,0:T(8,128)(2,1)S(1)} %slice_bitcast_fusion.refs_0_), channel_id=1, source_target_pairs={{0,2},{1,3},{2,0},{3,1},{4,6},{5,7},{6,4},{7,5},{8,10},{9,11},{10,... | collective-permute-start | bytes 1966088 | tf_op jit(solution)/shard_map/ppermute | solution.py:272
  69.7 50.7 %collective-permute-start.29 = (bf16[256,1280]{1,0:T(8,128)(2,1)S(1)}, bf16[256,1280]{1,0:T(8,128)(2,1)S(1)}, u32[]{:S(2)}, u32[]{:S(2)}) collective-permute-start(bf16[256,1280]{1,0:T(8,128)(2,1)S(1)} %slice_bitcast_fusion.refs_0_), channel_id=1, source_target_pairs={{0,1},{1,0},{2,3},{3,2},{4,5},{5,4},{6,7},{7,6},{8,9},{9,8},{10,11... | collective-permute-start | bytes 1966088 | tf_op jit(solution)/shard_map/ppermute | solution.py:272
  76.7 41.4 %collective-permute-start.20 = (bf16[256,768]{1,0:T(8,128)(2,1)S(1)}, bf16[256,768]{1,0:T(8,128)(2,1)S(1)}, u32[]{:S(2)}, u32[]{:S(2)}) collective-permute-start(bf16[256,768]{1,0:T(8,128)(2,1)S(1)} %slice_bitcast_fusion.1.refs_0_), channel_id=1, source_target_pairs={{0,2},{1,3},{2,0},{3,1},{4,6},{5,7},{6,4},{7,5},{8,10},{9,11},{10,... | collective-permute-start | bytes 1179656 | tf_op jit(solution)/shard_map/ppermute | solution.py:272
  118.1 8.6 %collective-permute-start.16 = (bf16[2048,256]{1,0:T(8,128)(2,1)S(1)}, bf16[2048,256]{1,0:T(8,128)(2,1)S(1)}, u32[]{:S(2)}, u32[]{:S(2)}) collective-permute-start(bf16[2048,256]{1,0:T(8,128)(2,1)S(1)} %bitcast.23), channel_id=1, source_target_pairs={{0,1},{1,0},{2,3},{3,2},{4,5},{5,4},{6,7},{7,6},{8,9},{9,8},{10,11... | collective-permute-start | bytes 3145736 | tf_op jit(solution)/shard_map/ppermute | solution.py:272
  118.7 8.6 %collective-permute-start.18 = (bf16[2048,256]{1,0:T(8,128)(2,1)S(1)}, bf16[2048,256]{1,0:T(8,128)(2,1)S(1)}, u32[]{:S(2)}, u32[]{:S(2)}) collective-permute-start(bf16[2048,256]{1,0:T(8,128)(2,1)S(1)} %collective-permute-done.17.refs_14_), channel_id=1, source_target_pairs={{0,1},{1,0},{2,3},{3,2},{4,5},{5,4},{6,7},{7,6},{8,9},{9,8},{10,11... | collective-permute-start | bytes 3145736 | tf_op jit(solution)/shard_map/ppermute | solution.py:272
  126.3 10.1 %collective-permute-start.19 = (bf16[256,768]{1,0:T(8,128)(2,1)S(1)}, bf16[256,768]{1,0:T(8,128)(2,1)S(1)}, u32[]{:S(2)}, u32[]{:S(2)}) collective-permute-start(bf16[256,768]{1,0:T(8,128)(2,1)S(1)} %slice_bitcast_fusion.1.refs_0_), channel_id=1, source_target_pairs={{0,1},{1,0},{2,3},{3,2},{4,5},{5,4},{6,7},{7,6},{8,9},{9,8},{10,11... | collective-permute-start | bytes 1179656 | tf_op jit(solution)/shard_map/ppermute | solution.py:272
  126.7 22.2 %collective-permute-start.3 = (bf16[128,2048]{1,0:T(8,128)(2,1)S(1)}, bf16[128,2048]{1,0:T(8,128)(2,1)S(1)}, u32[]{:S(2)}, u32[]{:S(2)}) collective-permute-start(bf16[128,2048]{1,0:T(8,128)(2,1)S(1)} %get-tuple-element.52), channel_id=1, source_target_pairs={{0,1},{1,0},{2,3},{3,2},{4,5},{5,4},{6,7},{7,6},{8,9},{9,8},{10,11... | collective-permute-start | bytes 1572872 | tf_op jit(solution)/shard_map/ppermute | solution.py:272
  126.9 20.4 %collective-permute-start.21 = (bf16[256,768]{1,0:T(8,128)(2,1)S(1)}, bf16[256,768]{1,0:T(8,128)(2,1)S(1)}, u32[]{:S(2)}, u32[]{:S(2)}) collective-permute-start(bf16[256,768]{1,0:T(8,128)(2,1)S(1)} %collective-permute-done.20.refs_2_), channel_id=1, source_target_pairs={{0,1},{1,0},{2,3},{3,2},{4,5},{5,4},{6,7},{7,6},{8,9},{9,8},{10,11... | collective-permute-start | bytes 1179656 | tf_op jit(solution)/shard_map/ppermute | solution.py:272
  127.3 21.7 %collective-permute-start.5 = (bf16[128,2048]{1,0:T(8,128)(2,1)S(1)}, bf16[128,2048]{1,0:T(8,128)(2,1)S(1)}, u32[]{:S(2)}, u32[]{:S(2)}) collective-permute-start(bf16[128,2048]{1,0:T(8,128)(2,1)S(1)} %add_convert_fusion.1), channel_id=1, source_target_pairs={{0,2},{1,3},{2,0},{3,1},{4,6},{5,7},{6,4},{7,5},{8,10},{9,11},{10,... | collective-permute-start | bytes 1572872 | tf_op jit(solution)/shard_map/ppermute | solution.py:272
  134.9 23.2 %collective-permute-start.32 = (bf16[64,1280]{1,0:T(8,128)(2,1)S(1)}, bf16[64,1280]{1,0:T(8,128)(2,1)S(1)}, u32[]{:S(2)}, u32[]{:S(2)}) collective-permute-start(bf16[64,1280]{1,0:T(8,128)(2,1)S(1)} %get-tuple-element.75), channel_id=1, source_target_pairs={{0,4},{4,0},{8,12},{12,8},{16,20},{20,16},{24,28},{28,24},{1,5},{5... | collective-permute-start | bytes 491528 | tf_op jit(solution)/shard_map/ppermute | solution.py:272
  136.4 23.8 %collective-permute-start.33 = (bf16[64,1280]{1,0:T(8,128)(2,1)S(1)}, bf16[64,1280]{1,0:T(8,128)(2,1)S(1)}, u32[]{:S(2)}, u32[]{:S(2)}) collective-permute-start(bf16[64,1280]{1,0:T(8,128)(2,1)S(1)} %get-tuple-element.76), channel_id=1, source_target_pairs={{0,8},{4,12},{8,0},{12,4},{16,24},{20,28},{24,16},{28,20},{1,9},{5... | collective-permute-start | bytes 491528 | tf_op jit(solution)/shard_map/ppermute | solution.py:272
  149.0 13.5 %collective-permute-start.34 = (bf16[64,1280]{1,0:T(8,128)(2,1)S(1)}, bf16[64,1280]{1,0:T(8,128)(2,1)S(1)}, u32[]{:S(2)}, u32[]{:S(2)}) collective-permute-start(bf16[64,1280]{1,0:T(8,128)(2,1)S(1)} %get-tuple-element.77), channel_id=1, source_target_pairs={{0,12},{4,8},{8,4},{12,0},{16,28},{20,24},{24,20},{28,16},{1,13},{... | collective-permute-start | bytes 491528 | tf_op jit(solution)/shard_map/ppermute | solution.py:272
  153.0 23.2 %collective-permute-start.35 = (bf16[64,1280]{1,0:T(8,128)(2,1)S(1)}, bf16[64,1280]{1,0:T(8,128)(2,1)S(1)}, u32[]{:S(2)}, u32[]{:S(2)}) collective-permute-start(bf16[64,1280]{1,0:T(8,128)(2,1)S(1)} %get-tuple-element.78), channel_id=1, source_target_pairs={{0,16},{4,20},{8,24},{12,28},{16,0},{20,4},{24,8},{28,12},{1,17},{... | collective-permute-start | bytes 491528 | tf_op jit(solution)/shard_map/ppermute | solution.py:272
  156.7 21.6 %collective-permute-start.36 = (bf16[64,1280]{1,0:T(8,128)(2,1)S(1)}, bf16[64,1280]{1,0:T(8,128)(2,1)S(1)}, u32[]{:S(2)}, u32[]{:S(2)}) collective-permute-start(bf16[64,1280]{1,0:T(8,128)(2,1)S(1)} %get-tuple-element.79), channel_id=1, source_target_pairs={{0,20},{4,16},{8,28},{12,24},{16,4},{20,0},{24,12},{28,8},{1,21},{... | collective-permute-start | bytes 491528 | tf_op jit(solution)/shard_map/ppermute | solution.py:272
  158.1 20.2 %collective-permute-start.37 = (bf16[64,1280]{1,0:T(8,128)(2,1)S(1)}, bf16[64,1280]{1,0:T(8,128)(2,1)S(1)}, u32[]{:S(2)}, u32[]{:S(2)}) collective-permute-start(bf16[64,1280]{1,0:T(8,128)(2,1)S(1)} %get-tuple-element.80), channel_id=1, source_target_pairs={{0,24},{4,28},{8,16},{12,20},{16,8},{20,12},{24,0},{28,4},{1,25},{... | collective-permute-start | bytes 491528 | tf_op jit(solution)/shard_map/ppermute | solution.py:272
  160.2 24.6 %collective-permute-start.38 = (bf16[64,1280]{1,0:T(8,128)(2,1)S(1)}, bf16[64,1280]{1,0:T(8,128)(2,1)S(1)}, u32[]{:S(2)}, u32[]{:S(2)}) collective-permute-start(bf16[64,1280]{1,0:T(8,128)(2,1)S(1)} %get-tuple-element.81), channel_id=1, source_target_pairs={{0,28},{4,24},{8,20},{12,16},{16,12},{20,8},{24,4},{28,0},{1,29},{... | collective-permute-start | bytes 491528 | tf_op jit(solution)/shard_map/ppermute | solution.py:272
  162.4 25.9 %collective-permute-start.24 = (bf16[64,768]{1,0:T(8,128)(2,1)S(1)}, bf16[64,768]{1,0:T(8,128)(2,1)S(1)}, u32[]{:S(2)}, u32[]{:S(2)}) collective-permute-start(bf16[64,768]{1,0:T(8,128)(2,1)S(1)} %get-tuple-element.69), channel_id=1, source_target_pairs={{0,12},{4,8},{8,4},{12,0},{16,28},{20,24},{24,20},{28,16},{1,13},{... | collective-permute-start | bytes 294920 | tf_op jit(solution)/shard_map/ppermute | solution.py:272
  176.2 20.4 %collective-permute-start.25 = (bf16[64,768]{1,0:T(8,128)(2,1)S(1)}, bf16[64,768]{1,0:T(8,128)(2,1)S(1)}, u32[]{:S(2)}, u32[]{:S(2)}) collective-permute-start(bf16[64,768]{1,0:T(8,128)(2,1)S(1)} %get-tuple-element.70), channel_id=1, source_target_pairs={{0,16},{4,20},{8,24},{12,28},{16,0},{20,4},{24,8},{28,12},{1,17},{... | collective-permute-start | bytes 294920 | tf_op jit(solution)/shard_map/ppermute | solution.py:272
  178.3 19.7 %collective-permute-start.26 = (bf16[64,768]{1,0:T(8,128)(2,1)S(1)}, bf16[64,768]{1,0:T(8,128)(2,1)S(1)}, u32[]{:S(2)}, u32[]{:S(2)}) collective-permute-start(bf16[64,768]{1,0:T(8,128)(2,1)S(1)} %get-tuple-element.71), channel_id=1, source_target_pairs={{0,20},{4,16},{8,28},{12,24},{16,4},{20,0},{24,12},{28,8},{1,21},{... | collective-permute-start | bytes 294920 | tf_op jit(solution)/shard_map/ppermute | solution.py:272
  178.3 19.7 %collective-permute-start.27 = (bf16[64,768]{1,0:T(8,128)(2,1)S(1)}, bf16[64,768]{1,0:T(8,128)(2,1)S(1)}, u32[]{:S(2)}, u32[]{:S(2)}) collective-permute-start(bf16[64,768]{1,0:T(8,128)(2,1)S(1)} %get-tuple-element.72), channel_id=1, source_target_pairs={{0,24},{4,28},{8,16},{12,20},{16,8},{20,12},{24,0},{28,4},{1,25},{... | collective-permute-start | bytes 294920 | tf_op jit(solution)/shard_map/ppermute | solution.py:272
  184.8 13.1 %collective-permute-start.28 = (bf16[64,768]{1,0:T(8,128)(2,1)S(1)}, bf16[64,768]{1,0:T(8,128)(2,1)S(1)}, u32[]{:S(2)}, u32[]{:S(2)}) collective-permute-start(bf16[64,768]{1,0:T(8,128)(2,1)S(1)} %get-tuple-element.73), channel_id=1, source_target_pairs={{0,28},{4,24},{8,20},{12,16},{16,12},{20,8},{24,4},{28,0},{1,29},{... | collective-permute-start | bytes 294920 | tf_op jit(solution)/shard_map/ppermute | solution.py:272
  (23 other events, 492.9 us)

commit v2 on v1

--- a/solution.py
+++ b/solution.py
@@ -11,7 +11,7 @@
 CHUNK = 128
 FINE = 16
 DIRECT_EP = 8
-DOWN_EIGHTHS = (5, 3)
+DOWN_EIGHTHS = (3, 3, 2)
 TILE = 256
 F32 = jnp.float32
 BF16 = jnp.bfloat16
@@ -297,10 +297,21 @@
     return sums[0].astype(BF16)
 
 
-def routing_kernel(groups, experts, me_ref, quarter_ref, rows_ref, gain_ref, routes_ref, *outs):
-    count, _ = rows_ref.shape
+def routing_kernel(groups, experts, count, me_ref, quarter_ref, rows_hbm, gain_hbm, routes_hbm, *refs):
+    outs = refs[:groups]
+    rows_ref, gain_ref, routes_ref, sems = refs[groups:]
     slots = 2 * TOPK * count // experts
     per_group = experts * slots // groups
+    start = pl.multiple_of(quarter_ref[0] * count, count)
+    copies = [
+        pltpu.make_async_copy(rows_hbm.at[pl.ds(start, count)], rows_ref, sems.at[0]),
+        pltpu.make_async_copy(routes_hbm.at[:, pl.ds(start, count)], routes_ref, sems.at[1]),
+        pltpu.make_async_copy(gain_hbm, gain_ref, sems.at[2]),
+    ]
+    for one in copies:
+        one.start()
+    for one in copies:
+        one.wait()
     wide = rows_ref[...].astype(F32)
     square = jnp.mean(wide * wide, axis=-1, keepdims=True)
     normed = (wide * lax.rsqrt(square + EPS) * gain_ref[...]).astype(BF16)
@@ -444,23 +455,19 @@
     parts = list(zip(edges, edges[1:]))
     downs = [gather_quarters(expert_down_matrix[0, :, start:stop], "tp") for start, stop in parts]
 
-    def whole(grid_index, a, b):
-        return (0, 0)
-
     outgoing = call(
-        functools.partial(routing_kernel, groups, ep),
+        functools.partial(routing_kernel, groups, ep, count),
         (me, quarter, second_residual, expert_norm_scale.reshape(1, -1), routes_t),
-        grid_spec=pltpu.PrefetchScalarGridSpec(
-            num_scalar_prefetch=2,
-            grid=(1,),
-            in_specs=[
-                pl.BlockSpec((count, model), lambda i, a, b: (b[0], 0)),
-                pl.BlockSpec((1, model), whole),
-                pl.BlockSpec((TOPK, count), lambda i, a, b: (0, b[0])),
-            ],
-            out_specs=[pl.BlockSpec((per_group, model), whole)] * groups,
-        ),
+        room=60,
+        in_specs=[SM, SM, HBM, HBM, HBM],
+        out_specs=[VM] * groups,
         out_shape=[shape((per_group, model), BF16)] * groups,
+        scratch_shapes=[
+            pltpu.VMEM((count, model), BF16),
+            pltpu.VMEM((1, model), F32),
+            pltpu.VMEM((TOPK, count), routes.dtype),
+            pltpu.SemaphoreType.DMA((3,)),
+        ],
         cost_estimate=cost(2 * capacity * count * model, 2 * (count + capacity) * model),
     )
 
@@ -564,6 +571,9 @@
     )
     mixer_output = scatter_sum(mixed, "tp")
 
+    def whole(grid_index, a, b):
+        return (0, 0)
+
     pick, weight = call(
         functools.partial(picks_kernel, groups, ep),
         (me, quarter, routes_t, factor_t),

time: 201 us -> 173 us (0.86); the launches traced: 199 us -> 173 us
  waiting for transfers between devices: 99.5 us -> 74.8 us
  local copies, waits for them, and re-layouts: 8.03 us -> 0.18 us
  starting transfers between devices: 73.8 us -> 78.1 us
  Pallas kernels: 15.7 us -> 17.9 us
    ppermute x39 -> x49, waiting for transfers between devices: 99.5 us -> 74.8 us  [swap(): lax.ppermute(array, axis, [(place, place ^ bit) for place in range(size)])]
    unnamed x32 -> x42, local copies, waits for them, and re-layouts: 5.88 us -> 0.11 us
    ppermute x39 -> x49, starting transfers between devices: 73.8 us -> 78.1 us  [swap(): lax.ppermute(array, axis, [(place, place ^ bit) for place in range(size)])]
    pallas_call x11 -> x13, Pallas kernels: 15.7 us -> 17.9 us  [call(): pl.pallas_call(kernel, compiler_params=params(room), **options)(*operands)]
    squeeze x2, local copies, waits for them, and re-layouts: 2.15 us -> 0.07 us  [shards(): expert_down_matrix[0, :, start:stop]]
  transfers between devices with their start and end apart: 39 -> 49, of which waited for: 9 -> 15; matrix products, arithmetic and copies ran while one was open for 2% -> 1% of each run, Pallas kernels for 6% -> 8%
where the time goes in v2:
time: 173 us
  starting transfers between devices  78.1 us (45%)
  waiting for transfers between devices  74.8 us (43%)
  Pallas kernels  17.9 us (10%)
    ppermute x49, starting transfers between devices, swap(): lax.ppermute(array, axis, [(place, place ^ bit) for place in range(size)])  78.1 us
    ppermute x49, waiting for transfers between devices, swap(): lax.ppermute(array, axis, [(place, place ^ bit) for place in range(size)])  74.8 us
    pallas_call x13, Pallas kernels, call(): pl.pallas_call(kernel, compiler_params=params(room), **options)(*operands)  17.9 us
  transfers between devices with their start and end apart: 49, of which 15 were waited for; matrix products, arithmetic and copies ran while one was open for 1% of the time, Pallas kernels for 8%

profile of v2, /device:TPU:0, one launch (start us, length us, event | category | flops | bytes accessed | tf_op | source)
XLA Modules:
  0.0 173.2 jit_solution(6752714187700887703)
XLA Ops:
  0.7 3.8 %shard_map.181 = (bf16[64,2048]{1,0:T(8,128)(2,1)}, bf16[64,2048]{1,0:T(8,128)(2,1)}, bf16[64,2048]{1,0:T(8,128)(2,1)}, bf16[64,2048]{1,0:T(8,128)(2,1)}, bf16[6...) custom-call(s32[1]{0:T(128)} %bitcast.me_ref, ...), custom_call_target="tpu_custom_call" | custom-call | flops 268435456 | bytes 2621440 | tf_op jit(solution)/shard_map/pallas_call | solution.py:414
  4.5 5.1 %collective-permute-start.10 = (bf16[64,2048]{1,0:T(8,128)(2,1)}, bf16[64,2048]{1,0:T(8,128)(2,1)S(1)}, u32[]{:S(2)}, u32[]{:S(2)}) collective-permute-start(bf16[64,2048]{1,0:T(8,128)(2,1)} %get-tuple-element.71), channel_id=1, source_target_pairs={{0,20},{4,16},{8,28},{12,24},{16,4},{20,0},{24,12},{28,8},{1,21},{... | collective-permute-start | bytes 786440 | tf_op jit(solution)/shard_map/ppermute | solution.py:272
  11.0 3.0 %shard_map.177 = (f32[512,256]{1,0:T(8,128)S(1)}, bf16[512,256]{1,0:T(8,128)(2,1)S(1)}, bf16[512,256]{1,0:T(8,128)(2,1)S(1)}, bf16[2,272,128]{2,1,0:T(8,128)(2,1)S(1)}) custom-call(bf16[512,256]{1,0:T(8,128)(2,1)S(1)} %copy-done.6, bf16[512,256]{1,0:T(8,128)(2,1)S(1)} %copy-done.7, bf16[512,256]{1,0:T(8,128)(2,1)S(1)} %copy-done.8, ...), custom_call_target="tpu_custom_call" | custom-call | flops 12000000000 | bytes 1048576 | tf_op jit(solution)/shard_map/pallas_call | solution.py:414
  14.7 3.4 %collective-permute-start.12 = (bf16[64,2048]{1,0:T(8,128)(2,1)S(1)}, bf16[64,2048]{1,0:T(8,128)(2,1)S(1)}, u32[]{:S(2)}, u32[]{:S(2)}) collective-permute-start(bf16[64,2048]{1,0:T(8,128)(2,1)S(1)} %copy-done.20), channel_id=1, source_target_pairs={{0,28},{4,24},{8,20},{12,16},{16,12},{20,8},{24,4},{28,0},{1,29},{... | collective-permute-start | bytes 786440 | tf_op jit(solution)/shard_map/ppermute | solution.py:272
  19.2 2.2 %collective-permute-start.7 = (bf16[64,2048]{1,0:T(8,128)(2,1)S(1)}, bf16[64,2048]{1,0:T(8,128)(2,1)S(1)}, u32[]{:S(2)}, u32[]{:S(2)}) collective-permute-start(bf16[64,2048]{1,0:T(8,128)(2,1)S(1)} %copy-done.18), channel_id=1, source_target_pairs={{0,8},{4,12},{8,0},{12,4},{16,24},{20,28},{24,16},{28,20},{1,9},{5... | collective-permute-start | bytes 786440 | tf_op jit(solution)/shard_map/ppermute | solution.py:272
  21.4 12.5 %collective-permute-done.10.refs_5_ = bf16[64,2048]{1,0:T(8,128)(2,1)S(1)} collective-permute-done((bf16[64,2048]{1,0:T(8,128)(2,1)}, bf16[64,2048]{1,0:T(8,128)(2,1)S(1)}, u32[]{:S(2)}, u32[]{:S(2)}) %collective-permute-start.10) | collective-permute-done | bytes 262176 | tf_op jit(solution)/shard_map/ppermute | solution.py:272
  33.9 1.8 %collective-permute-start.14 = (bf16[2048,256]{1,0:T(8,128)(2,1)S(1)}, bf16[2048,256]{1,0:T(8,128)(2,1)S(1)}, u32[]{:S(2)}, u32[]{:S(2)}) collective-permute-start(bf16[2048,256]{1,0:T(8,128)(2,1)S(1)} %bitcast.20), channel_id=1, source_target_pairs={{0,2},{1,3},{2,0},{3,1},{4,6},{5,7},{6,4},{7,5},{8,10},{9,11},{10,... | collective-permute-start | bytes 3145736 | tf_op jit(solution)/shard_map/ppermute | solution.py:272
  35.9 9.9 %collective-permute-start.8 = (bf16[64,2048]{1,0:T(8,128)(2,1)S(1)}, bf16[64,2048]{1,0:T(8,128)(2,1)S(1)}, u32[]{:S(2)}, u32[]{:S(2)}) collective-permute-start(bf16[64,2048]{1,0:T(8,128)(2,1)S(1)} %copy-done.17), channel_id=1, source_target_pairs={{0,12},{4,8},{8,4},{12,0},{16,28},{20,24},{24,20},{28,16},{1,13},{... | collective-permute-start | bytes 786440 | tf_op jit(solution)/shard_map/ppermute | solution.py:272
  47.0 2.9 %collective-permute-start.1 = (bf16[2,272,128]{2,1,0:T(8,128)(2,1)S(1)}, bf16[2,272,128]{2,1,0:T(8,128)(2,1)S(1)}, u32[]{:S(2)}, u32[]{:S(2)}) collective-permute-start(bf16[2,272,128]{2,1,0:T(8,128)(2,1)S(1)} %get-tuple-element.55.own_ref), channel_id=1, source_target_pairs={{0,8},{4,12},{8,0},{12,4},{16,24},{20,28},{24,16},{28,20},{1,9},{5... | collective-permute-start | bytes 417800 | tf_op jit(solution)/shard_map/ppermute | solution.py:272
  50.0 8.5 %collective-permute-done.8.refs_3_ = bf16[64,2048]{1,0:T(8,128)(2,1)S(1)} collective-permute-done((bf16[64,2048]{1,0:T(8,128)(2,1)S(1)}, bf16[64,2048]{1,0:T(8,128)(2,1)S(1)}, u32[]{:S(2)}, u32[]{:S(2)}) %collective-permute-start.8) | collective-permute-done | bytes 262176 | tf_op jit(solution)/shard_map/ppermute | solution.py:272
  60.4 4.6 %collective-permute-start.2 = (bf16[272,128]{1,0:T(8,128)(2,1)S(1)}, bf16[272,128]{1,0:T(8,128)(2,1)S(1)}, u32[]{:S(2)}, u32[]{:S(2)}) collective-permute-start(bf16[272,128]{1,0:T(8,128)(2,1)S(1)} %get-tuple-element.57), channel_id=1, source_target_pairs={{0,16},{4,20},{8,24},{12,28},{16,0},{20,4},{24,8},{28,12},{1,17},{... | collective-permute-start | bytes 208904 | tf_op jit(solution)/shard_map/ppermute | solution.py:272
  65.1 20.4 %collective-permute-done.20.refs_2_ = bf16[256,512]{1,0:T(8,128)(2,1)S(1)} collective-permute-done((bf16[256,512]{1,0:T(8,128)(2,1)S(1)}, bf16[256,512]{1,0:T(8,128)(2,1)S(1)}, u32[]{:S(2)}, u32[]{:S(2)}) %collective-permute-start.20) | collective-permute-done | bytes 262176 | tf_op jit(solution)/shard_map/ppermute | solution.py:272
  85.4 1.7 collective-permute-start.40
  87.5 9.9 %collective-permute-done.40.refs_2_ = bf16[256,768]{1,0:T(8,128)(2,1)S(1)} collective-permute-done((bf16[256,768]{1,0:T(8,128)(2,1)S(1)}, bf16[256,768]{1,0:T(8,128)(2,1)S(1)}, u32[]{:S(2)}, u32[]{:S(2)}) %collective-permute-start.40) | collective-permute-done | bytes 393248 | tf_op jit(solution)/shard_map/ppermute | solution.py:272
  99.7 2.7 %collective-permute-done.30.refs_2_ = bf16[256,768]{1,0:T(8,128)(2,1)S(1)} collective-permute-done((bf16[256,768]{1,0:T(8,128)(2,1)S(1)}, bf16[256,768]{1,0:T(8,128)(2,1)S(1)}, u32[]{:S(2)}, u32[]{:S(2)}) %collective-permute-start.30) | collective-permute-done | bytes 393248 | tf_op jit(solution)/shard_map/ppermute | solution.py:272
  102.4 2.9 %collective-permute-done.4 = bf16[128,2048]{1,0:T(8,128)(2,1)S(1)} collective-permute-done((bf16[128,2048]{1,0:T(8,128)(2,1)S(1)}, bf16[128,2048]{1,0:T(8,128)(2,1)S(1)}, u32[]{:S(2)}, u32[]{:S(2)}) %collective-permute-start.4) | collective-permute-done | bytes 524320 | tf_op jit(solution)/shard_map/ppermute | solution.py:272
  107.9 1.7 collective-permute-start.5
  109.6 4.5 %shard_map.182.hidden_ref = bf16[512,1024]{1,0:T(8,128)(2,1)S(1)} custom-call(bf16[64,2048]{1,0:T(8,128)(2,1)S(1)} %copy-done.10, bf16[64,2048]{1,0:T(8,128)(2,1)S(1)} %collective-permute-done.6.refs_1_, bf16[64,2048]{1,0:T(8,128)(2,1)S(1)} %collective-permute-done.7.refs_2_, bf16[64,2048]{1,0:T(8,128)(2,1)S(1)} %collective-permute-done.8.refs_3_, ...), custom_call_target="tpu_custom_call" | custom-call | flops 4294967296 | bytes 8388608 | tf_op jit(solution)/shard_map/pallas_call | solution.py:414
  118.0 2.0 %collective-permute-start.43 = (bf16[64,768]{1,0:T(8,128)(2,1)S(1)}, bf16[64,768]{1,0:T(8,128)(2,1)S(1)}, u32[]{:S(2)}, u32[]{:S(2)}) collective-permute-start(bf16[64,768]{1,0:T(8,128)(2,1)S(1)} %get-tuple-element.92), channel_id=1, source_target_pairs={{0,8},{4,12},{8,0},{12,4},{16,24},{20,28},{24,16},{28,20},{1,9},{5... | collective-permute-start | bytes 294920 | tf_op jit(solution)/shard_map/ppermute | solution.py:272
  121.9 2.3 %collective-permute-start.45 = (bf16[64,768]{1,0:T(8,128)(2,1)S(1)}, bf16[64,768]{1,0:T(8,128)(2,1)S(1)}, u32[]{:S(2)}, u32[]{:S(2)}) collective-permute-start(bf16[64,768]{1,0:T(8,128)(2,1)S(1)} %get-tuple-element.94), channel_id=1, source_target_pairs={{0,16},{4,20},{8,24},{12,28},{16,0},{20,4},{24,8},{28,12},{1,17},{... | collective-permute-start | bytes 294920 | tf_op jit(solution)/shard_map/ppermute | solution.py:272
  124.2 3.0 %collective-permute-start.23 = (bf16[64,512]{1,0:T(8,128)(2,1)S(1)}, bf16[64,512]{1,0:T(8,128)(2,1)S(1)}, u32[]{:S(2)}, u32[]{:S(2)}) collective-permute-start(bf16[64,512]{1,0:T(8,128)(2,1)S(1)} %get-tuple-element.76), channel_id=1, source_target_pairs={{0,8},{4,12},{8,0},{12,4},{16,24},{20,28},{24,16},{28,20},{1,9},{5... | collective-permute-start | bytes 196616 | tf_op jit(solution)/shard_map/ppermute | solution.py:272
  129.5 2.9 %collective-permute-start.46 = (bf16[64,768]{1,0:T(8,128)(2,1)S(1)}, bf16[64,768]{1,0:T(8,128)(2,1)S(1)}, u32[]{:S(2)}, u32[]{:S(2)}) collective-permute-start(bf16[64,768]{1,0:T(8,128)(2,1)S(1)} %get-tuple-element.95), channel_id=1, source_target_pairs={{0,20},{4,16},{8,28},{12,24},{16,4},{20,0},{24,12},{28,8},{1,21},{... | collective-permute-start | bytes 294920 | tf_op jit(solution)/shard_map/ppermute | solution.py:272
  132.3 2.4 %collective-permute-start.47 = (bf16[64,768]{1,0:T(8,128)(2,1)S(1)}, bf16[64,768]{1,0:T(8,128)(2,1)S(1)}, u32[]{:S(2)}, u32[]{:S(2)}) collective-permute-start(bf16[64,768]{1,0:T(8,128)(2,1)S(1)} %get-tuple-element.96), channel_id=1, source_target_pairs={{0,24},{4,28},{8,16},{12,20},{16,8},{20,12},{24,0},{28,4},{1,25},{... | collective-permute-start | bytes 294920 | tf_op jit(solution)/shard_map/ppermute | solution.py:272
  134.8 1.9 %collective-permute-start.48 = (bf16[64,768]{1,0:T(8,128)(2,1)S(1)}, bf16[64,768]{1,0:T(8,128)(2,1)S(1)}, u32[]{:S(2)}, u32[]{:S(2)}) collective-permute-start(bf16[64,768]{1,0:T(8,128)(2,1)S(1)} %get-tuple-element.97), channel_id=1, source_target_pairs={{0,28},{4,24},{8,20},{12,16},{16,12},{20,8},{24,4},{28,0},{1,29},{... | collective-permute-start | bytes 294920 | tf_op jit(solution)/shard_map/ppermute | solution.py:272
  137.7 3.6 %collective-permute-done.46.refs_5_ = bf16[64,768]{1,0:T(8,128)(2,1)S(1)} collective-permute-done((bf16[64,768]{1,0:T(8,128)(2,1)S(1)}, bf16[64,768]{1,0:T(8,128)(2,1)S(1)}, u32[]{:S(2)}, u32[]{:S(2)}) %collective-permute-start.46) | collective-permute-done | bytes 98336 | tf_op jit(solution)/shard_map/ppermute | solution.py:272
  141.2 5.4 %collective-permute-start.35 = (bf16[64,768]{1,0:T(8,128)(2,1)S(1)}, bf16[64,768]{1,0:T(8,128)(2,1)S(1)}, u32[]{:S(2)}, u32[]{:S(2)}) collective-permute-start(bf16[64,768]{1,0:T(8,128)(2,1)S(1)} %get-tuple-element.86), channel_id=1, source_target_pairs={{0,16},{4,20},{8,24},{12,28},{16,0},{20,4},{24,8},{28,12},{1,17},{... | collective-permute-start | bytes 294920 | tf_op jit(solution)/shard_map/ppermute | solution.py:272
  146.7 4.1 %collective-permute-start.36 = (bf16[64,768]{1,0:T(8,128)(2,1)S(1)}, bf16[64,768]{1,0:T(8,128)(2,1)S(1)}, u32[]{:S(2)}, u32[]{:S(2)}) collective-permute-start(bf16[64,768]{1,0:T(8,128)(2,1)S(1)} %get-tuple-element.87), channel_id=1, source_target_pairs={{0,20},{4,16},{8,28},{12,24},{16,4},{20,0},{24,12},{28,8},{1,21},{... | collective-permute-start | bytes 294920 | tf_op jit(solution)/shard_map/ppermute | solution.py:272
  151.3 3.7 %collective-permute-start.38 = (bf16[64,768]{1,0:T(8,128)(2,1)S(1)}, bf16[64,768]{1,0:T(8,128)(2,1)S(1)}, u32[]{:S(2)}, u32[]{:S(2)}) collective-permute-start(bf16[64,768]{1,0:T(8,128)(2,1)S(1)} %get-tuple-element.89), channel_id=1, source_target_pairs={{0,28},{4,24},{8,20},{12,16},{16,12},{20,8},{24,4},{28,0},{1,29},{... | collective-permute-start | bytes 294920 | tf_op jit(solution)/shard_map/ppermute | solution.py:272
  155.6 4.6 %collective-permute-done.35.refs_4_ = bf16[64,768]{1,0:T(8,128)(2,1)S(1)} collective-permute-done((bf16[64,768]{1,0:T(8,128)(2,1)S(1)}, bf16[64,768]{1,0:T(8,128)(2,1)S(1)}, u32[]{:S(2)}, u32[]{:S(2)}) %collective-permute-start.35) | collective-permute-done | bytes 98336 | tf_op jit(solution)/shard_map/ppermute | solution.py:272
  160.2 3.2 %collective-permute-done.36.refs_5_ = bf16[64,768]{1,0:T(8,128)(2,1)S(1)} collective-permute-done((bf16[64,768]{1,0:T(8,128)(2,1)S(1)}, bf16[64,768]{1,0:T(8,128)(2,1)S(1)}, u32[]{:S(2)}, u32[]{:S(2)}) %collective-permute-start.36) | collective-permute-done | bytes 98336 | tf_op jit(solution)/shard_map/ppermute | solution.py:272
  164.6 3.3 %collective-permute-start.28 = (bf16[64,512]{1,0:T(8,128)(2,1)S(1)}, bf16[64,512]{1,0:T(8,128)(2,1)S(1)}, u32[]{:S(2)}, u32[]{:S(2)}) collective-permute-start(bf16[64,512]{1,0:T(8,128)(2,1)S(1)} %get-tuple-element.81), channel_id=1, source_target_pairs={{0,28},{4,24},{8,20},{12,16},{16,12},{20,8},{24,4},{28,0},{1,29},{... | collective-permute-start | bytes 196616 | tf_op jit(solution)/shard_map/ppermute | solution.py:272
  170.1 2.0 %collective-permute-done.26.refs_5_ = bf16[64,512]{1,0:T(8,128)(2,1)S(1)} collective-permute-done((bf16[64,512]{1,0:T(8,128)(2,1)S(1)}, bf16[64,512]{1,0:T(8,128)(2,1)S(1)}, u32[]{:S(2)}, u32[]{:S(2)}) %collective-permute-start.26) | collective-permute-done | bytes 65568 | tf_op jit(solution)/shard_map/ppermute | solution.py:272
  (125 shorter events, 26.5 us)
Async XLA Ops:
  4.5 29.4 %collective-permute-start.10 = (bf16[64,2048]{1,0:T(8,128)(2,1)}, bf16[64,2048]{1,0:T(8,128)(2,1)S(1)}, u32[]{:S(2)}, u32[]{:S(2)}) collective-permute-start(bf16[64,2048]{1,0:T(8,128)(2,1)} %get-tuple-element.71), channel_id=1, source_target_pairs={{0,20},{4,16},{8,28},{12,24},{16,4},{20,0},{24,12},{28,8},{1,21},{... | collective-permute-start | bytes 786440 | tf_op jit(solution)/shard_map/ppermute | solution.py:272
  9.6 26.1 %collective-permute-start.11 = (bf16[64,2048]{1,0:T(8,128)(2,1)}, bf16[64,2048]{1,0:T(8,128)(2,1)S(1)}, u32[]{:S(2)}, u32[]{:S(2)}) collective-permute-start(bf16[64,2048]{1,0:T(8,128)(2,1)} %get-tuple-element.72), channel_id=1, source_target_pairs={{0,24},{4,28},{8,16},{12,20},{16,8},{20,12},{24,0},{28,4},{1,25},{... | collective-permute-start | bytes 786440 | tf_op jit(solution)/shard_map/ppermute | solution.py:272
  14.7 21.2 %collective-permute-start.12 = (bf16[64,2048]{1,0:T(8,128)(2,1)S(1)}, bf16[64,2048]{1,0:T(8,128)(2,1)S(1)}, u32[]{:S(2)}, u32[]{:S(2)}) collective-permute-start(bf16[64,2048]{1,0:T(8,128)(2,1)S(1)} %copy-done.20), channel_id=1, source_target_pairs={{0,28},{4,24},{8,20},{12,16},{16,12},{20,8},{24,4},{28,0},{1,29},{... | collective-permute-start | bytes 786440 | tf_op jit(solution)/shard_map/ppermute | solution.py:272
  18.1 27.6 %collective-permute-start.6 = (bf16[64,2048]{1,0:T(8,128)(2,1)S(1)}, bf16[64,2048]{1,0:T(8,128)(2,1)S(1)}, u32[]{:S(2)}, u32[]{:S(2)}) collective-permute-start(bf16[64,2048]{1,0:T(8,128)(2,1)S(1)} %copy-done.19), channel_id=1, source_target_pairs={{0,4},{4,0},{8,12},{12,8},{16,20},{20,16},{24,28},{28,24},{1,5},{5... | collective-permute-start | bytes 786440 | tf_op jit(solution)/shard_map/ppermute | solution.py:272
  19.2 27.8 %collective-permute-start.7 = (bf16[64,2048]{1,0:T(8,128)(2,1)S(1)}, bf16[64,2048]{1,0:T(8,128)(2,1)S(1)}, u32[]{:S(2)}, u32[]{:S(2)}) collective-permute-start(bf16[64,2048]{1,0:T(8,128)(2,1)S(1)} %copy-done.18), channel_id=1, source_target_pairs={{0,8},{4,12},{8,0},{12,4},{16,24},{20,28},{24,16},{28,20},{1,9},{5... | collective-permute-start | bytes 786440 | tf_op jit(solution)/shard_map/ppermute | solution.py:272
  33.9 64.1 %collective-permute-start.14 = (bf16[2048,256]{1,0:T(8,128)(2,1)S(1)}, bf16[2048,256]{1,0:T(8,128)(2,1)S(1)}, u32[]{:S(2)}, u32[]{:S(2)}) collective-permute-start(bf16[2048,256]{1,0:T(8,128)(2,1)S(1)} %bitcast.20), channel_id=1, source_target_pairs={{0,2},{1,3},{2,0},{3,1},{4,6},{5,7},{6,4},{7,5},{8,10},{9,11},{10,... | collective-permute-start | bytes 3145736 | tf_op jit(solution)/shard_map/ppermute | solution.py:272
  35.7 62.3 %collective-permute-start.17 = (bf16[2048,256]{1,0:T(8,128)(2,1)S(1)}, bf16[2048,256]{1,0:T(8,128)(2,1)S(1)}, u32[]{:S(2)}, u32[]{:S(2)}) collective-permute-start(bf16[2048,256]{1,0:T(8,128)(2,1)S(1)} %bitcast.23), channel_id=1, source_target_pairs={{0,2},{1,3},{2,0},{3,1},{4,6},{5,7},{6,4},{7,5},{8,10},{9,11},{10,... | collective-permute-start | bytes 3145736 | tf_op jit(solution)/shard_map/ppermute | solution.py:272
  35.9 22.6 %collective-permute-start.8 = (bf16[64,2048]{1,0:T(8,128)(2,1)S(1)}, bf16[64,2048]{1,0:T(8,128)(2,1)S(1)}, u32[]{:S(2)}, u32[]{:S(2)}) collective-permute-start(bf16[64,2048]{1,0:T(8,128)(2,1)S(1)} %copy-done.17), channel_id=1, source_target_pairs={{0,12},{4,8},{8,4},{12,0},{16,28},{20,24},{24,20},{28,16},{1,13},{... | collective-permute-start | bytes 786440 | tf_op jit(solution)/shard_map/ppermute | solution.py:272
  45.8 14.6 %collective-permute-start.9 = (bf16[64,2048]{1,0:T(8,128)(2,1)S(1)}, bf16[64,2048]{1,0:T(8,128)(2,1)S(1)}, u32[]{:S(2)}, u32[]{:S(2)}) collective-permute-start(bf16[64,2048]{1,0:T(8,128)(2,1)S(1)} %copy-done.16), channel_id=1, source_target_pairs={{0,16},{4,20},{8,24},{12,28},{16,0},{20,4},{24,8},{28,12},{1,17},{... | collective-permute-start | bytes 786440 | tf_op jit(solution)/shard_map/ppermute | solution.py:272
  47.0 13.0 %collective-permute-start.1 = (bf16[2,272,128]{2,1,0:T(8,128)(2,1)S(1)}, bf16[2,272,128]{2,1,0:T(8,128)(2,1)S(1)}, u32[]{:S(2)}, u32[]{:S(2)}) collective-permute-start(bf16[2,272,128]{2,1,0:T(8,128)(2,1)S(1)} %get-tuple-element.55.own_ref), channel_id=1, source_target_pairs={{0,8},{4,12},{8,0},{12,4},{16,24},{20,28},{24,16},{28,20},{1,9},{5... | collective-permute-start | bytes 417800 | tf_op jit(solution)/shard_map/ppermute | solution.py:272
  58.5 26.9 %collective-permute-start.20 = (bf16[256,512]{1,0:T(8,128)(2,1)S(1)}, bf16[256,512]{1,0:T(8,128)(2,1)S(1)}, u32[]{:S(2)}, u32[]{:S(2)}) collective-permute-start(bf16[256,512]{1,0:T(8,128)(2,1)S(1)} %slice_bitcast_fusion.2.refs_0_), channel_id=1, source_target_pairs={{0,2},{1,3},{2,0},{3,1},{4,6},{5,7},{6,4},{7,5},{8,10},{9,11},{10,... | collective-permute-start | bytes 786440 | tf_op jit(solution)/shard_map/ppermute | solution.py:272
  60.1 27.0 %collective-permute-start.19 = (bf16[256,512]{1,0:T(8,128)(2,1)S(1)}, bf16[256,512]{1,0:T(8,128)(2,1)S(1)}, u32[]{:S(2)}, u32[]{:S(2)}) collective-permute-start(bf16[256,512]{1,0:T(8,128)(2,1)S(1)} %slice_bitcast_fusion.2.refs_0_), channel_id=1, source_target_pairs={{0,1},{1,0},{2,3},{3,2},{4,5},{5,4},{6,7},{7,6},{8,9},{9,8},{10,11... | collective-permute-start | bytes 786440 | tf_op jit(solution)/shard_map/ppermute | solution.py:272
  60.4 26.7 %collective-permute-start.2 = (bf16[272,128]{1,0:T(8,128)(2,1)S(1)}, bf16[272,128]{1,0:T(8,128)(2,1)S(1)}, u32[]{:S(2)}, u32[]{:S(2)}) collective-permute-start(bf16[272,128]{1,0:T(8,128)(2,1)S(1)} %get-tuple-element.57), channel_id=1, source_target_pairs={{0,16},{4,20},{8,24},{12,28},{16,0},{20,4},{24,8},{28,12},{1,17},{... | collective-permute-start | bytes 208904 | tf_op jit(solution)/shard_map/ppermute | solution.py:272
  85.4 12.0 %collective-permute-start.40 = (bf16[256,768]{1,0:T(8,128)(2,1)S(1)}, bf16[256,768]{1,0:T(8,128)(2,1)S(1)}, u32[]{:S(2)}, u32[]{:S(2)}) collective-permute-start(bf16[256,768]{1,0:T(8,128)(2,1)S(1)} %get-tuple-element.98.refs_0_), channel_id=1, source_target_pairs={{0,2},{1,3},{2,0},{3,1},{4,6},{5,7},{6,4},{7,5},{8,10},{9,11},{10,... | collective-permute-start | bytes 1179656 | tf_op jit(solution)/shard_map/ppermute | solution.py:272
  87.1 15.3 %collective-permute-start.30 = (bf16[256,768]{1,0:T(8,128)(2,1)S(1)}, bf16[256,768]{1,0:T(8,128)(2,1)S(1)}, u32[]{:S(2)}, u32[]{:S(2)}) collective-permute-start(bf16[256,768]{1,0:T(8,128)(2,1)S(1)} %get-tuple-element.99.refs_0_), channel_id=1, source_target_pairs={{0,2},{1,3},{2,0},{3,1},{4,6},{5,7},{6,4},{7,5},{8,10},{9,11},{10,... | collective-permute-start | bytes 1179656 | tf_op jit(solution)/shard_map/ppermute | solution.py:272
  106.9 10.5 %collective-permute-start.29 = (bf16[256,768]{1,0:T(8,128)(2,1)S(1)}, bf16[256,768]{1,0:T(8,128)(2,1)S(1)}, u32[]{:S(2)}, u32[]{:S(2)}) collective-permute-start(bf16[256,768]{1,0:T(8,128)(2,1)S(1)} %get-tuple-element.99.refs_0_), channel_id=1, source_target_pairs={{0,1},{1,0},{2,3},{3,2},{4,5},{5,4},{6,7},{7,6},{8,9},{9,8},{10,11... | collective-permute-start | bytes 1179656 | tf_op jit(solution)/shard_map/ppermute | solution.py:272
  107.0 13.0 %collective-permute-start.3 = (bf16[128,2048]{1,0:T(8,128)(2,1)S(1)}, bf16[128,2048]{1,0:T(8,128)(2,1)S(1)}, u32[]{:S(2)}, u32[]{:S(2)}) collective-permute-start(bf16[128,2048]{1,0:T(8,128)(2,1)S(1)} %get-tuple-element.60), channel_id=1, source_target_pairs={{0,1},{1,0},{2,3},{3,2},{4,5},{5,4},{6,7},{7,6},{8,9},{9,8},{10,11... | collective-permute-start | bytes 1572872 | tf_op jit(solution)/shard_map/ppermute | solution.py:272
  107.9 14.0 %collective-permute-start.5 = (bf16[128,2048]{1,0:T(8,128)(2,1)S(1)}, bf16[128,2048]{1,0:T(8,128)(2,1)S(1)}, u32[]{:S(2)}, u32[]{:S(2)}) collective-permute-start(bf16[128,2048]{1,0:T(8,128)(2,1)S(1)} %add_convert_fusion.1), channel_id=1, source_target_pairs={{0,2},{1,3},{2,0},{3,1},{4,6},{5,7},{6,4},{7,5},{8,10},{9,11},{10,... | collective-permute-start | bytes 1572872 | tf_op jit(solution)/shard_map/ppermute | solution.py:272
  117.4 15.0 %collective-permute-start.42 = (bf16[64,768]{1,0:T(8,128)(2,1)S(1)}, bf16[64,768]{1,0:T(8,128)(2,1)S(1)}, u32[]{:S(2)}, u32[]{:S(2)}) collective-permute-start(bf16[64,768]{1,0:T(8,128)(2,1)S(1)} %get-tuple-element.91), channel_id=1, source_target_pairs={{0,4},{4,0},{8,12},{12,8},{16,20},{20,16},{24,28},{28,24},{1,5},{5... | collective-permute-start | bytes 294920 | tf_op jit(solution)/shard_map/ppermute | solution.py:272
  118.0 16.8 %collective-permute-start.43 = (bf16[64,768]{1,0:T(8,128)(2,1)S(1)}, bf16[64,768]{1,0:T(8,128)(2,1)S(1)}, u32[]{:S(2)}, u32[]{:S(2)}) collective-permute-start(bf16[64,768]{1,0:T(8,128)(2,1)S(1)} %get-tuple-element.92), channel_id=1, source_target_pairs={{0,8},{4,12},{8,0},{12,4},{16,24},{20,28},{24,16},{28,20},{1,9},{5... | collective-permute-start | bytes 294920 | tf_op jit(solution)/shard_map/ppermute | solution.py:272
  120.0 16.7 %collective-permute-start.44 = (bf16[64,768]{1,0:T(8,128)(2,1)S(1)}, bf16[64,768]{1,0:T(8,128)(2,1)S(1)}, u32[]{:S(2)}, u32[]{:S(2)}) collective-permute-start(bf16[64,768]{1,0:T(8,128)(2,1)S(1)} %get-tuple-element.93), channel_id=1, source_target_pairs={{0,12},{4,8},{8,4},{12,0},{16,28},{20,24},{24,20},{28,16},{1,13},{... | collective-permute-start | bytes 294920 | tf_op jit(solution)/shard_map/ppermute | solution.py:272
  121.9 15.8 %collective-permute-start.45 = (bf16[64,768]{1,0:T(8,128)(2,1)S(1)}, bf16[64,768]{1,0:T(8,128)(2,1)S(1)}, u32[]{:S(2)}, u32[]{:S(2)}) collective-permute-start(bf16[64,768]{1,0:T(8,128)(2,1)S(1)} %get-tuple-element.94), channel_id=1, source_target_pairs={{0,16},{4,20},{8,24},{12,28},{16,0},{20,4},{24,8},{28,12},{1,17},{... | collective-permute-start | bytes 294920 | tf_op jit(solution)/shard_map/ppermute | solution.py:272
  129.5 11.8 %collective-permute-start.46 = (bf16[64,768]{1,0:T(8,128)(2,1)S(1)}, bf16[64,768]{1,0:T(8,128)(2,1)S(1)}, u32[]{:S(2)}, u32[]{:S(2)}) collective-permute-start(bf16[64,768]{1,0:T(8,128)(2,1)S(1)} %get-tuple-element.95), channel_id=1, source_target_pairs={{0,20},{4,16},{8,28},{12,24},{16,4},{20,0},{24,12},{28,8},{1,21},{... | collective-permute-start | bytes 294920 | tf_op jit(solution)/shard_map/ppermute | solution.py:272
  134.8 11.9 %collective-permute-start.48 = (bf16[64,768]{1,0:T(8,128)(2,1)S(1)}, bf16[64,768]{1,0:T(8,128)(2,1)S(1)}, u32[]{:S(2)}, u32[]{:S(2)}) collective-permute-start(bf16[64,768]{1,0:T(8,128)(2,1)S(1)} %get-tuple-element.97), channel_id=1, source_target_pairs={{0,28},{4,24},{8,20},{12,16},{16,12},{20,8},{24,4},{28,0},{1,29},{... | collective-permute-start | bytes 294920 | tf_op jit(solution)/shard_map/ppermute | solution.py:272
  136.6 14.1 %collective-permute-start.32 = (bf16[64,768]{1,0:T(8,128)(2,1)S(1)}, bf16[64,768]{1,0:T(8,128)(2,1)S(1)}, u32[]{:S(2)}, u32[]{:S(2)}) collective-permute-start(bf16[64,768]{1,0:T(8,128)(2,1)S(1)} %get-tuple-element.83), channel_id=1, source_target_pairs={{0,4},{4,0},{8,12},{12,8},{16,20},{20,16},{24,28},{28,24},{1,5},{5... | collective-permute-start | bytes 294920 | tf_op jit(solution)/shard_map/ppermute | solution.py:272
  137.6 13.7 %collective-permute-start.33 = (bf16[64,768]{1,0:T(8,128)(2,1)S(1)}, bf16[64,768]{1,0:T(8,128)(2,1)S(1)}, u32[]{:S(2)}, u32[]{:S(2)}) collective-permute-start(bf16[64,768]{1,0:T(8,128)(2,1)S(1)} %get-tuple-element.84), channel_id=1, source_target_pairs={{0,8},{4,12},{8,0},{12,4},{16,24},{20,28},{24,16},{28,20},{1,9},{5... | collective-permute-start | bytes 294920 | tf_op jit(solution)/shard_map/ppermute | solution.py:272
  141.2 14.3 %collective-permute-start.34 = (bf16[64,768]{1,0:T(8,128)(2,1)S(1)}, bf16[64,768]{1,0:T(8,128)(2,1)S(1)}, u32[]{:S(2)}, u32[]{:S(2)}) collective-permute-start(bf16[64,768]{1,0:T(8,128)(2,1)S(1)} %get-tuple-element.85), channel_id=1, source_target_pairs={{0,12},{4,8},{8,4},{12,0},{16,28},{20,24},{24,20},{28,16},{1,13},{... | collective-permute-start | bytes 294920 | tf_op jit(solution)/shard_map/ppermute | solution.py:272
  141.2 18.9 %collective-permute-start.35 = (bf16[64,768]{1,0:T(8,128)(2,1)S(1)}, bf16[64,768]{1,0:T(8,128)(2,1)S(1)}, u32[]{:S(2)}, u32[]{:S(2)}) collective-permute-start(bf16[64,768]{1,0:T(8,128)(2,1)S(1)} %get-tuple-element.86), channel_id=1, source_target_pairs={{0,16},{4,20},{8,24},{12,28},{16,0},{20,4},{24,8},{28,12},{1,17},{... | collective-permute-start | bytes 294920 | tf_op jit(solution)/shard_map/ppermute | solution.py:272
  146.7 16.7 %collective-permute-start.36 = (bf16[64,768]{1,0:T(8,128)(2,1)S(1)}, bf16[64,768]{1,0:T(8,128)(2,1)S(1)}, u32[]{:S(2)}, u32[]{:S(2)}) collective-permute-start(bf16[64,768]{1,0:T(8,128)(2,1)S(1)} %get-tuple-element.87), channel_id=1, source_target_pairs={{0,20},{4,16},{8,28},{12,24},{16,4},{20,0},{24,12},{28,8},{1,21},{... | collective-permute-start | bytes 294920 | tf_op jit(solution)/shard_map/ppermute | solution.py:272
  150.7 12.8 %collective-permute-start.37 = (bf16[64,768]{1,0:T(8,128)(2,1)S(1)}, bf16[64,768]{1,0:T(8,128)(2,1)S(1)}, u32[]{:S(2)}, u32[]{:S(2)}) collective-permute-start(bf16[64,768]{1,0:T(8,128)(2,1)S(1)} %get-tuple-element.88), channel_id=1, source_target_pairs={{0,24},{4,28},{8,16},{12,20},{16,8},{20,12},{24,0},{28,4},{1,25},{... | collective-permute-start | bytes 294920 | tf_op jit(solution)/shard_map/ppermute | solution.py:272
  151.3 13.2 %collective-permute-start.38 = (bf16[64,768]{1,0:T(8,128)(2,1)S(1)}, bf16[64,768]{1,0:T(8,128)(2,1)S(1)}, u32[]{:S(2)}, u32[]{:S(2)}) collective-permute-start(bf16[64,768]{1,0:T(8,128)(2,1)S(1)} %get-tuple-element.89), channel_id=1, source_target_pairs={{0,28},{4,24},{8,20},{12,16},{16,12},{20,8},{24,4},{28,0},{1,29},{... | collective-permute-start | bytes 294920 | tf_op jit(solution)/shard_map/ppermute | solution.py:272
  155.5 14.1 %collective-permute-start.24 = (bf16[64,512]{1,0:T(8,128)(2,1)S(1)}, bf16[64,512]{1,0:T(8,128)(2,1)S(1)}, u32[]{:S(2)}, u32[]{:S(2)}) collective-permute-start(bf16[64,512]{1,0:T(8,128)(2,1)S(1)} %get-tuple-element.77), channel_id=1, source_target_pairs={{0,12},{4,8},{8,4},{12,0},{16,28},{20,24},{24,20},{28,16},{1,13},{... | collective-permute-start | bytes 196616 | tf_op jit(solution)/shard_map/ppermute | solution.py:272
  (38 other events, 711.8 us)
